TPU v7x, 32 devices: a whole 2x2x4 slice. The times are simulated.
32 devices in a mesh: fs: 4 (over z), rep: 4 (over y, x), tp: 2 (over core).
Axes of the slice: x: 2, y: 2, z: 4, core: 2. Of those that a mesh axis runs over, the one named last changes fastest.
Arguments:
- normed_input: bfloat16 [2048, 1024], P(('fs', 'rep')), may hold values from -6 to 6
- query_cotangent: bfloat16 [2048, 512], P(('fs', 'rep'), 'tp'), may hold values from -0.029907227 to 0.029907227
- value_cotangent: bfloat16 [2048, 1024], P(('fs', 'rep'), 'tp'), may hold values from -0.029907227 to 0.029907227
- query_basis: bfloat16 [1024, 128], replicated, may hold values from -0.1875 to 0.1875
- value_basis: bfloat16 [1024, 128], replicated, may hold values from -0.1875 to 0.1875
- query_weight: float32 [1024, 512], P(('fs', 'rep'), 'tp'), may hold values from -0.1875 to 0.1875
- value_weight: float32 [1024, 1024], P(('fs', 'rep'), 'tp'), may hold values from -0.1875 to 0.1875
- query_first: float32 [128, 512], P(('fs', 'rep'), 'tp'), may hold values from -6 to 6
- query_second: float32 [128, 512], P(('fs', 'rep'), 'tp'), may hold values from 0.25 to 4
- value_first: float32 [128, 1024], P(('fs', 'rep'), 'tp'), may hold values from -6 to 6
- value_second: float32 [128, 1024], P(('fs', 'rep'), 'tp'), may hold values from 0.25 to 4
Outputs:
- query_update: float32 [1024, 512], P(('fs', 'rep'), 'tp')
- value_update: float32 [1024, 1024], P(('fs', 'rep'), 'tp')
- query_weight_new: float32 [1024, 512], P(('fs', 'rep'), 'tp')
- value_weight_new: float32 [1024, 1024], P(('fs', 'rep'), 'tp')
- query_first_new: float32 [128, 512], P(('fs', 'rep'), 'tp')
- query_second_new: float32 [128, 512], P(('fs', 'rep'), 'tp')
- value_first_new: float32 [128, 1024], P(('fs', 'rep'), 'tp')
- value_second_new: float32 [128, 1024], P(('fs', 'rep'), 'tp')
- query_copy: bfloat16 [1024, 512], P(None, 'tp')
- value_copy: bfloat16 [1024, 1024], P(None, 'tp')
All inputs are finite; a program needn't handle non-finite values.
Results may differ from a plain program's by a relative error of at most 0.001.
Values may be sent and summed in bfloat16 or wider, within the bound.
No kernel may reach another device: no remote copies, remote signals or barrier semaphores. Data moves between devices by JAX's collectives and lax.ppermute only.
A program may use at most 64 MiB of HBM per device.

v0:
```python
import functools

import jax
import jax.numpy as jnp
from jax import lax
from jax.experimental import pallas as pl
from jax.experimental.pallas import tpu as pltpu
from jax.sharding import PartitionSpec as P


F32, BF16 = jnp.float32, jnp.bfloat16
VMEM = pl.BlockSpec(memory_space=pltpu.VMEM)
SMEM = pl.BlockSpec(memory_space=pltpu.SMEM)
ANY = pl.BlockSpec(memory_space=pltpu.MemorySpace.HBM)
PARAMS = pltpu.CompilerParams(vmem_limit_bytes=16 * 2**20)


def swap(block, axis, mask):
    count = lax.axis_size(axis)
    pairs = [(i, i ^ mask) for i in range(count)]
    return lax.ppermute(block, axis, pairs)


def spread(block, axis):
    return [block] + [swap(block, axis, k) for k in range(1, lax.axis_size(axis))]


def in_order(blocks, own):
    stacked = jnp.stack(blocks)
    return jnp.stack(
        [lax.dynamic_index_in_dim(stacked, j ^ own, 0, keepdims=False) for j in range(len(blocks))]
    )


def split_parts(wide):
    high_part = wide.astype(BF16)
    held = lax.optimization_barrier(high_part)
    low_part = (wide - held.astype(F32)).astype(BF16)
    return (high_part, low_part)


def parts_product(high_part, low_part, cotangent):
    dims = (((0,), (0,)), ((), ()))
    first_term = lax.dot_general(high_part, cotangent, dims, preferred_element_type=F32)
    second_term = lax.dot_general(low_part, cotangent, dims, preferred_element_type=F32)
    return first_term + second_term


def moments(projected, first_old, second_old):
    first_new = 0.9 * first_old + 0.1 * projected
    second_new = 0.99 * second_old + 0.01 * projected * projected
    return (first_new, second_new, first_new / (jnp.sqrt(second_new) + 1e-08))


def aligned(start, size):
    return pl.ds(pl.multiple_of(start * size, size), size)


def stage_kernel(query_weight, value_weight, query_first, value_first, *refs):
    query_second, value_second, weights, own, sems = refs
    rows, ranks = query_weight.shape[0], query_first.shape[0]
    query_width, width = query_weight.shape[1], weights.shape[1]
    copies = []
    for target, left, right, low in (
        (weights, query_weight, value_weight, 0),
        (own, query_weight, value_weight, 0),
        (own, query_first, value_first, rows),
        (own, query_second, value_second, rows + ranks),
    ):
        for source, columns in ((left, pl.ds(0, query_width)), (right, pl.ds(query_width, width - query_width))):
            copies.append(
                pltpu.make_async_copy(
                    source, target.at[pl.ds(low, source.shape[0]), columns], sems.at[len(copies)]
                )
            )
    for copy in copies:
        copy.start()
    for copy in copies:
        copy.wait()


def project_kernel(counts, place, *refs):
    fs, rep, ranks = counts
    sources, chunks, total = refs[:5], refs[5 : 5 + rep], refs[5 + rep]
    tokens, query_basis, value_basis, query_cot, value_cot = held = refs[6 + rep : 11 + rep]
    sems = refs[11 + rep]
    copies = [
        pltpu.make_async_copy(source, target, sems.at[i])
        for i, (source, target) in enumerate(zip(sources, held))
    ]
    for copy in copies:
        copy.start()
    for copy in copies:
        copy.wait()
    r = place[1]
    query_width = query_cot.shape[1]
    for basis, cot, lo in ((query_basis, query_cot, 0), (value_basis, value_cot, query_width)):
        reduced = jnp.dot(tokens[...], basis[...], preferred_element_type=F32)
        high = reduced.astype(BF16)
        low = (reduced - high.astype(F32)).astype(BF16)
        total[:, lo : lo + cot.shape[1]] = parts_product(high, low, cot[...])
    for k in range(rep):
        for zz in range(fs):
            chunks[k][zz * ranks : (zz + 1) * ranks, :] = total[
                aligned(zz * rep + (r ^ k), ranks), :
            ]


def moments_kernel(counts, place, mine, other, *refs):
    fs, rows, ranks, query_width = counts
    blocks, (query_first, query_second, value_first, value_second, direction) = refs[:fs], refs[fs:]
    z = place[0]
    for k in range(fs):
        where = aligned(z ^ k, ranks)
        first, second, ratio = moments(
            mine[where, :] + other[where, :],
            blocks[k][rows : rows + ranks, :],
            blocks[k][rows + ranks : rows + 2 * ranks, :],
        )
        direction[where, :] = ratio
        if k == 0:
            query_first[...] = first[:, :query_width]
            query_second[...] = second[:, :query_width]
            value_first[...] = first[:, query_width:]
            value_second[...] = second[:, query_width:]


def whole_kernel(counts, place, *refs):
    fs, rep, ranks, query_width = counts
    blocks, (whole, sums) = refs[:rep], refs[rep:]
    r = place[1]
    for k in range(rep):
        for zz in range(fs):
            whole[aligned(zz * rep + (r ^ k), ranks), :] = blocks[k][
                zz * ranks : (zz + 1) * ranks, :
            ]
    squares = whole[0:ranks, :] * whole[0:ranks, :]
    for row in range(1, fs * rep):
        part = whole[row * ranks : (row + 1) * ranks, :]
        squares = squares + part * part
    query_sum = jnp.sum(squares[:, :query_width], keepdims=True)
    value_sum = jnp.sum(squares[:, query_width:], keepdims=True)
    sums[0:1, :] = jnp.broadcast_to(query_sum, (1, sums.shape[1]))
    sums[1:2, :] = jnp.broadcast_to(value_sum, (1, sums.shape[1]))


def product_kernel(whole, query_basis, value_basis, query_product, value_product):
    query_width = query_product.shape[1]
    for basis, product, lo in (
        (query_basis, query_product, 0),
        (value_basis, value_product, query_width),
    ):
        wide = whole[:, lo : lo + product.shape[1]]
        high = wide.astype(BF16)
        low = (wide - high.astype(F32)).astype(BF16)
        product[...] = jnp.dot(basis[...], high, preferred_element_type=F32) + jnp.dot(
            basis[...], low, preferred_element_type=F32
        )


def finish_kernel(counts, place, sums, query_product, value_product, *refs):
    fs, rep, rows, entries = counts
    blocks = refs[: fs * rep]
    query_update, value_update, query_new, value_new, query_copy, value_copy = refs[fs * rep :]
    z, r = place[0], place[1]
    query_width = query_product.shape[1]
    query_scale = 1.0 / jnp.sqrt(sums[0:1, 0:1] / entries[0] + 1.0)
    value_scale = 1.0 / jnp.sqrt(sums[1:2, 0:1] / entries[1] + 1.0)
    for kz in range(fs):
        for kr in range(rep):
            where = aligned((z ^ kz) * rep + (r ^ kr), rows)
            held = blocks[kz * rep + kr]
            for product, scale, lo, update, new, copy in (
                (query_product, query_scale, 0, query_update, query_new, query_copy),
                (value_product, value_scale, query_width, value_update, value_new, value_copy),
            ):
                step = product[where, :] * scale
                weight = held[:, lo : lo + product.shape[1]] - 0.01 * step
                copy[where, :] = weight.astype(BF16)
                if kz == 0 and kr == 0:
                    update[...] = step
                    new[...] = weight


def kernel_body(
    normed_input,
    query_cotangent,
    value_cotangent,
    query_basis,
    value_basis,
    query_weight,
    value_weight,
    query_first,
    query_second,
    value_first,
    value_second,
):
    fs, rep, tp = lax.axis_size("fs"), lax.axis_size("rep"), lax.axis_size("tp")
    place = jnp.stack([lax.axis_index("fs"), lax.axis_index("rep")]).astype(jnp.int32)
    rows, ranks = query_weight.shape[0], query_first.shape[0]
    query_width, value_width = query_cotangent.shape[1], value_cotangent.shape[1]
    width = query_width + value_width
    total = fs * rep * rows

    def shape(*dims, dtype=F32):
        return jax.ShapeDtypeStruct(dims, dtype)

    def call(kernel, out_shape, *operands, scratch=(), outside=()):
        specs = [SMEM if operand is place else VMEM for operand in operands]
        specs = [ANY if i in outside else spec for i, spec in enumerate(specs)]
        operands = [
            pltpu.with_memory_space_constraint(operand, pltpu.HBM) if i in outside else operand
            for i, operand in enumerate(operands)
        ]
        return pl.pallas_call(
            kernel,
            out_shape=out_shape,
            in_specs=specs,
            out_specs=jax.tree.map(lambda _: VMEM, out_shape),
            scratch_shapes=scratch,
            compiler_params=PARAMS,
        )(*operands)

    weights, own = call(
        stage_kernel,
        (shape(rows, width), shape(rows + 2 * ranks, width)),
        query_weight,
        value_weight,
        query_first,
        value_first,
        query_second,
        value_second,
        scratch=[pltpu.SemaphoreType.DMA((8,))],
        outside=range(6),
    )
    plane = spread(weights, "rep")
    along = spread(own, "fs")

    operands = (normed_input, query_basis, value_basis, query_cotangent, value_cotangent)
    chunks = call(
        functools.partial(project_kernel, (fs, rep, ranks)),
        (shape(fs * ranks, width),) * rep,
        place,
        *operands,
        scratch=[pltpu.VMEM((fs * rep * ranks, width), F32)]
        + [pltpu.VMEM(operand.shape, operand.dtype) for operand in operands]
        + [pltpu.SemaphoreType.DMA((5,))],
        outside=range(1, 6),
    )
    arrived = [swap(chunks[k], "rep", k) for k in range(1, rep)]
    mine = functools.reduce(jnp.add, arrived, chunks[0])
    far = []
    for k in range(1, fs):
        cut = along[k][:rows]
        far.append(spread(cut, "rep"))
    step = 1
    while 2 * step < fs:
        arrived = swap(mine, "fs", step)
        mine = mine + arrived
        step *= 2
    other = swap(mine, "fs", step)

    *new_moments, direction = call(
        functools.partial(moments_kernel, (fs, rows, ranks, query_width)),
        (shape(ranks, query_width),) * 2
        + (shape(ranks, value_width),) * 2
        + (shape(fs * ranks, width),),
        place,
        mine,
        other,
        *along,
    )
    whole, sums = call(
        functools.partial(whole_kernel, (fs, rep, ranks, query_width)),
        (shape(fs * rep * ranks, width), shape(2, 128)),
        place,
        *spread(direction, "rep"),
    )
    if tp == 2:
        sums = sums + swap(sums, "tp", 1)
    else:
        sums = lax.psum(sums, "tp")
    products = call(
        product_kernel,
        (shape(total, query_width), shape(total, value_width)),
        whole,
        query_basis,
        value_basis,
    )
    held = plane + sum(far, [])
    entries = (fs * rep * ranks * query_width * tp, fs * rep * ranks * value_width * tp)
    query_update, value_update, query_new, value_new, query_copy, value_copy = call(
        functools.partial(finish_kernel, (fs, rep, rows, entries)),
        (shape(rows, query_width), shape(rows, value_width)) * 2
        + (shape(total, query_width, dtype=BF16), shape(total, value_width, dtype=BF16)),
        place,
        sums,
        *products,
        *held,
    )
    query_first_new, query_second_new, value_first_new, value_second_new = new_moments
    return (
        query_update,
        value_update,
        query_new,
        value_new,
        query_first_new,
        query_second_new,
        value_first_new,
        value_second_new,
        query_copy,
        value_copy,
    )


def plain_body(
    normed_input,
    query_cotangent,
    value_cotangent,
    query_basis,
    value_basis,
    query_weight,
    value_weight,
    query_first,
    query_second,
    value_first,
    value_second,
):
    fs, rep, tp = lax.axis_size("fs"), lax.axis_size("rep"), lax.axis_size("tp")
    z, r = lax.axis_index("fs"), lax.axis_index("rep")
    rows = query_weight.shape[0]
    query_width, value_width = query_cotangent.shape[1], value_cotangent.shape[1]
    width = query_width + value_width
    total = fs * rep * rows

    weights = jnp.concatenate([query_weight, value_weight], axis=1)
    copies = in_order(spread(weights, "fs"), z)
    copies = in_order(spread(copies, "rep"), r).transpose(1, 0, 2, 3).reshape(total, width)
    partial = jnp.concatenate(
        [
            parts_product(
                *split_parts(jnp.dot(normed_input, basis, preferred_element_type=F32)), cotangent
            )
            for basis, cotangent in ((query_basis, query_cotangent), (value_basis, value_cotangent))
        ],
        axis=1,
    )
    projected = lax.psum_scatter(partial, ("fs", "rep"), scatter_dimension=0, tiled=True)
    first_new, second_new, direction = moments(
        projected,
        jnp.concatenate([query_first, value_first], axis=1),
        jnp.concatenate([query_second, value_second], axis=1),
    )
    whole = lax.all_gather(direction, ("fs", "rep"), axis=0, tiled=True)
    squares = whole * whole
    sums = lax.psum(
        jnp.stack([jnp.sum(squares[:, :query_width]), jnp.sum(squares[:, query_width:])]), "tp"
    )
    outs = []
    place = (z * rep + r) * rows
    for basis, lo, hi, squared in (
        (query_basis, 0, query_width, sums[0]),
        (value_basis, query_width, width, sums[1]),
    ):
        scale = jnp.sqrt(squared / (whole.shape[0] * (hi - lo) * tp) + 1.0)
        update = jnp.dot(basis.astype(F32), whole[:, lo:hi], precision=lax.Precision.HIGHEST) / scale
        new = copies[:, lo:hi] - 0.01 * update
        outs.append(lax.dynamic_slice_in_dim(update, place, rows, 0))
        outs.append(lax.dynamic_slice_in_dim(new, place, rows, 0))
        outs.append(new.astype(BF16))
    query_update, query_new, query_copy, value_update, value_new, value_copy = outs
    return (
        query_update,
        value_update,
        query_new,
        value_new,
        first_new[:, :query_width],
        second_new[:, :query_width],
        first_new[:, query_width:],
        second_new[:, query_width:],
        query_copy,
        value_copy,
    )


def body(*operands):
    query_weight, value_weight, query_first = operands[5:8]
    fits = query_first.shape[0] % 8 == 0 and query_weight.shape[0] % 16 == 0
    fits = fits and query_weight.shape[1] % 128 == 0 and value_weight.shape[1] % 128 == 0
    if fits and lax.axis_size("fs") >= 4:
        return kernel_body(*operands)
    return plain_body(*operands)


def solution(mesh):
    rows = P(("fs", "rep"), "tp")
    in_specs = (P(("fs", "rep"), None), rows, rows, P(), P()) + (rows,) * 6
    out_specs = (rows,) * 8 + (P(None, "tp"),) * 2
    return jax.shard_map(body, mesh=mesh, in_specs=in_specs, out_specs=out_specs, check_vma=False)
```

profile of v0, /device:TPU:0, one launch (start us, length us, event | category | flops | bytes accessed | tf_op | source)
XLA Modules:
  0.0 76.6 jit_solution(3105933804571806157)
XLA Ops:
  0.6 0.1 pad_add_fusion.place
  0.7 2.5 %shard_map.186 = (f32[32,768]{1,0:T(8,128)S(1)}, f32[32,768]{1,0:T(8,128)S(1)}, f32[32,768]{1,0:T(8,128)S(1)}, f32[32,768]{1,0:T(8,128)S(1)}) custom-call(s32[2]{0:T(128)S(1)} %pad_add_fusion.place, bf16[128,1024]{1,0:T(8,128)(2,1)} %refs_0_.2, bf16[1024,128]{1,0:T(8,128)(2,1)} %query_basis.1, bf16[1024,128]{1,0:T(8,128)(2,1)} %value_basis.1, ...), custom_call_target="tpu_custom_call" | custom-call | tf_op jit(solution)/shard_map/pallas_call | solution.py:215
  3.2 0.0 copy-start
  3.2 0.0 copy-start.1
  3.3 3.0 %collective-permute-start = (f32[32,768]{1,0:T(8,128)S(1)}, f32[32,768]{1,0:T(8,128)S(1)}, u32[]{:S(2)}, u32[]{:S(2)}) collective-permute-start(f32[32,768]{1,0:T(8,128)S(1)} %get-tuple-element.32), channel_id=1, source_target_pairs={{0,2},{2,0},{4,6},{6,4},{1,3},{3,1},{5,7},{7,5},{8,10},{10,8},{12,... | collective-permute-start | bytes 294920 | tf_op jit(solution)/shard_map/ppermute | solution.py:21
  6.3 1.5 %collective-permute-start.1 = (f32[32,768]{1,0:T(8,128)S(1)}, f32[32,768]{1,0:T(8,128)S(1)}, u32[]{:S(2)}, u32[]{:S(2)}) collective-permute-start(f32[32,768]{1,0:T(8,128)S(1)} %get-tuple-element.33), channel_id=1, source_target_pairs={{0,4},{2,6},{4,0},{6,2},{1,5},{3,7},{5,1},{7,3},{8,12},{10,14},{12... | collective-permute-start | bytes 294920 | tf_op jit(solution)/shard_map/ppermute | solution.py:21
  7.8 0.0 collective-permute-start.2
  7.8 1.1 %shard_map.187 = (f32[64,768]{1,0:T(8,128)S(1)}, f32[80,768]{1,0:T(8,128)S(1)}) custom-call(f32[64,256]{1,0:T(8,128)} %query_weight.1, f32[64,512]{1,0:T(8,128)} %value_weight.1, f32[8,256]{1,0:T(8,128)} %query_first.1, f32[8,512]{1,0:T(8,128)} %value_first.1, f32[8,256]{1,0:T(8,128)} %refs_0_.3, f32[8,512]{1,0:T(8,128)} %refs_1_.3), custom_call_target="tpu_custom_call" | custom-call | tf_op jit(solution)/shard_map/pallas_call | solution.py:215
  9.0 4.1 %collective-permute-start.7 = (f32[80,768]{1,0:T(8,128)S(1)}, f32[80,768]{1,0:T(8,128)S(1)}, u32[]{:S(2)}, u32[]{:S(2)}) collective-permute-start(f32[80,768]{1,0:T(8,128)S(1)} %get-tuple-element.35.refs_0_), channel_id=1, source_target_pairs={{0,24},{8,16},{16,8},{24,0},{1,25},{9,17},{17,9},{25,1},{2,26},{10... | collective-permute-start | bytes 737288 | tf_op jit(solution)/shard_map/ppermute | solution.py:21
  13.1 0.0 collective-permute-start.6
  13.1 0.0 collective-permute-done
  13.1 0.6 collective-permute-start.5
  13.7 0.0 collective-permute-done.1
  13.7 0.0 collective-permute-done.2
  13.8 1.5 %collective-permute-start.3 = (f32[32,768]{1,0:T(8,128)S(1)}, f32[32,768]{1,0:T(8,128)S(1)}, u32[]{:S(2)}, u32[]{:S(2)}) collective-permute-start(f32[32,768]{1,0:T(8,128)S(1)} %add_add_fusion), channel_id=1, source_target_pairs={{0,8},{8,0},{16,24},{24,16},{1,9},{9,1},{17,25},{25,17},{2,10},{10... | collective-permute-start | bytes 294920 | tf_op jit(solution)/shard_map/ppermute | solution.py:21
  15.2 2.4 %collective-permute-start.14 = (f32[64,768]{1,0:T(8,128)S(1)}, f32[64,768]{1,0:T(8,128)S(1)}, u32[]{:S(2)}, u32[]{:S(2)}) collective-permute-start(f32[64,768]{1,0:T(8,128)S(1)} %get-tuple-element.41.refs_0_), channel_id=1, source_target_pairs={{0,6},{2,4},{4,2},{6,0},{1,7},{3,5},{5,3},{7,1},{8,14},{10,12},{12... | collective-permute-start | bytes 589832 | tf_op jit(solution)/shard_map/ppermute | solution.py:21
  17.7 12.5 %collective-permute-done.3 = f32[32,768]{1,0:T(8,128)S(1)} collective-permute-done((f32[32,768]{1,0:T(8,128)S(1)}, f32[32,768]{1,0:T(8,128)S(1)}, u32[]{:S(2)}, u32[]{:S(2)}) %collective-permute-start.3) | collective-permute-done | bytes 98336 | tf_op jit(solution)/shard_map/ppermute | solution.py:21
  30.2 1.4 %collective-permute-start.4 = (f32[32,768]{1,0:T(8,128)S(1)}, f32[32,768]{1,0:T(8,128)S(1)}, u32[]{:S(2)}, u32[]{:S(2)}) collective-permute-start(f32[32,768]{1,0:T(8,128)S(1)} %add.18.mine), channel_id=1, source_target_pairs={{0,16},{8,24},{16,0},{24,8},{1,17},{9,25},{17,1},{25,9},{2,18},{10... | collective-permute-start | bytes 294920 | tf_op jit(solution)/shard_map/ppermute | solution.py:21
  31.6 0.0 collective-permute-done.7.refs_3_
  31.6 1.5 %collective-permute-start.13 = (f32[64,768]{1,0:T(8,128)S(1)}, f32[64,768]{1,0:T(8,128)S(1)}, u32[]{:S(2)}, u32[]{:S(2)}) collective-permute-start(f32[64,768]{1,0:T(8,128)S(1)} %get-tuple-element.41.refs_0_), channel_id=1, source_target_pairs={{0,4},{2,6},{4,0},{6,2},{1,5},{3,7},{5,1},{7,3},{8,12},{10,14},{12... | collective-permute-start | bytes 589832 | tf_op jit(solution)/shard_map/ppermute | solution.py:21
  33.1 2.1 %collective-permute-done.6.refs_2_ = f32[80,768]{1,0:T(8,128)S(1)} collective-permute-done((f32[80,768]{1,0:T(8,128)S(1)}, f32[80,768]{1,0:T(8,128)S(1)}, u32[]{:S(2)}, u32[]{:S(2)}) %collective-permute-start.6) | collective-permute-done | bytes 245792 | tf_op jit(solution)/shard_map/ppermute | solution.py:21
  35.1 0.0 collective-permute-done.5.refs_1_
  35.1 1.2 %collective-permute-done.4.other = f32[32,768]{1,0:T(8,128)S(1)} collective-permute-done((f32[32,768]{1,0:T(8,128)S(1)}, f32[32,768]{1,0:T(8,128)S(1)}, u32[]{:S(2)}, u32[]{:S(2)}) %collective-permute-start.4) | collective-permute-done | bytes 98336 | tf_op jit(solution)/shard_map/ppermute | solution.py:21
  36.3 1.2 %shard_map.188 = (f32[8,256]{1,0:T(8,128)}, f32[8,256]{1,0:T(8,128)}, f32[8,512]{1,0:T(8,128)}, f32[8,512]{1,0:T(8,128)}, f32[32,768]{1,0:T(8,128)S(1)}) custom-call(s32[2]{0:T(128)S(1)} %pad_add_fusion.place, f32[32,768]{1,0:T(8,128)S(1)} %add.18.mine, f32[32,768]{1,0:T(8,128)S(1)} %collective-permute-done.4.other, ...), custom_call_target="tpu_custom_call" | custom-call | tf_op jit(solution)/shard_map/pallas_call | solution.py:215
  37.5 2.5 %collective-permute-start.10 = (f32[32,768]{1,0:T(8,128)S(1)}, f32[32,768]{1,0:T(8,128)S(1)}, u32[]{:S(2)}, u32[]{:S(2)}) collective-permute-start(f32[32,768]{1,0:T(8,128)S(1)} %get-tuple-element.36.refs_0_), channel_id=1, source_target_pairs={{0,6},{2,4},{4,2},{6,0},{1,7},{3,5},{5,3},{7,1},{8,14},{10,12},{12... | collective-permute-start | bytes 294920 | tf_op jit(solution)/shard_map/ppermute | solution.py:21
  39.9 0.5 collective-permute-start.9
  40.4 0.5 collective-permute-start.8
  41.0 0.0 collective-permute-done.14.refs_3_
  41.0 1.5 %collective-permute-start.12 = (f32[64,768]{1,0:T(8,128)S(1)}, f32[64,768]{1,0:T(8,128)S(1)}, u32[]{:S(2)}, u32[]{:S(2)}) collective-permute-start(f32[64,768]{1,0:T(8,128)S(1)} %get-tuple-element.41.refs_0_), channel_id=1, source_target_pairs={{0,2},{2,0},{4,6},{6,4},{1,3},{3,1},{5,7},{7,5},{8,10},{10,8},{12,... | collective-permute-start | bytes 589832 | tf_op jit(solution)/shard_map/ppermute | solution.py:21
  42.5 0.0 collective-permute-done.13.refs_2_
  42.5 1.6 %collective-permute-start.23 = (f32[64,768]{1,0:T(8,128)S(1)}, f32[64,768]{1,0:T(8,128)S(1)}, u32[]{:S(2)}, u32[]{:S(2)}) collective-permute-start(f32[64,768]{1,0:T(8,128)S(1)} %slice.14.refs_12_), channel_id=1, source_target_pairs={{0,6},{2,4},{4,2},{6,0},{1,7},{3,5},{5,3},{7,1},{8,14},{10,12},{12... | collective-permute-start | bytes 589832 | tf_op jit(solution)/shard_map/ppermute | solution.py:21
  44.1 0.0 collective-permute-done.10.refs_3_
  44.1 1.5 %collective-permute-start.22 = (f32[64,768]{1,0:T(8,128)S(1)}, f32[64,768]{1,0:T(8,128)S(1)}, u32[]{:S(2)}, u32[]{:S(2)}) collective-permute-start(f32[64,768]{1,0:T(8,128)S(1)} %slice.14.refs_12_), channel_id=1, source_target_pairs={{0,4},{2,6},{4,0},{6,2},{1,5},{3,7},{5,1},{7,3},{8,12},{10,14},{12... | collective-permute-start | bytes 589832 | tf_op jit(solution)/shard_map/ppermute | solution.py:21
  45.6 0.0 collective-permute-done.9.refs_2_
  45.6 1.5 %collective-permute-start.21 = (f32[64,768]{1,0:T(8,128)S(1)}, f32[64,768]{1,0:T(8,128)S(1)}, u32[]{:S(2)}, u32[]{:S(2)}) collective-permute-start(f32[64,768]{1,0:T(8,128)S(1)} %slice.14.refs_12_), channel_id=1, source_target_pairs={{0,2},{2,0},{4,6},{6,4},{1,3},{3,1},{5,7},{7,5},{8,10},{10,8},{12,... | collective-permute-start | bytes 589832 | tf_op jit(solution)/shard_map/ppermute | solution.py:21
  47.1 0.0 collective-permute-done.8.refs_1_
  47.1 0.7 collective-permute-start.20
  47.8 0.7 shard_map.189
  48.5 1.9 %collective-permute-done.12.refs_1_ = f32[64,768]{1,0:T(8,128)S(1)} collective-permute-done((f32[64,768]{1,0:T(8,128)S(1)}, f32[64,768]{1,0:T(8,128)S(1)}, u32[]{:S(2)}, u32[]{:S(2)}) %collective-permute-start.12) | collective-permute-done | bytes 196640 | tf_op jit(solution)/shard_map/ppermute | solution.py:21
  50.4 0.0 collective-permute-start.11
  50.4 1.1 %collective-permute-done.11 = f32[2,128]{1,0:T(2,128)S(1)} collective-permute-done((f32[2,128]{1,0:T(2,128)S(1)}, f32[2,128]{1,0:T(2,128)S(1)}, u32[]{:S(2)}, u32[]{:S(2)}) %collective-permute-start.11) | collective-permute-done | bytes 1056 | tf_op jit(solution)/shard_map/ppermute | solution.py:21
  51.6 1.4 %collective-permute-start.19 = (f32[64,768]{1,0:T(8,128)S(1)}, f32[64,768]{1,0:T(8,128)S(1)}, u32[]{:S(2)}, u32[]{:S(2)}) collective-permute-start(f32[64,768]{1,0:T(8,128)S(1)} %slice.13.refs_8_), channel_id=1, source_target_pairs={{0,4},{2,6},{4,0},{6,2},{1,5},{3,7},{5,1},{7,3},{8,12},{10,14},{12... | collective-permute-start | bytes 589832 | tf_op jit(solution)/shard_map/ppermute | solution.py:21
  53.0 2.5 %collective-permute-done.23.refs_15_ = f32[64,768]{1,0:T(8,128)S(1)} collective-permute-done((f32[64,768]{1,0:T(8,128)S(1)}, f32[64,768]{1,0:T(8,128)S(1)}, u32[]{:S(2)}, u32[]{:S(2)}) %collective-permute-start.23) | collective-permute-done | bytes 196640 | tf_op jit(solution)/shard_map/ppermute | solution.py:21
  55.5 0.6 collective-permute-start.18
  56.1 0.0 collective-permute-done.22.refs_14_
  56.1 1.5 %collective-permute-start.17 = (f32[64,768]{1,0:T(8,128)S(1)}, f32[64,768]{1,0:T(8,128)S(1)}, u32[]{:S(2)}, u32[]{:S(2)}) collective-permute-start(f32[64,768]{1,0:T(8,128)S(1)} %slice.12.refs_4_), channel_id=1, source_target_pairs={{0,6},{2,4},{4,2},{6,0},{1,7},{3,5},{5,3},{7,1},{8,14},{10,12},{12... | collective-permute-start | bytes 589832 | tf_op jit(solution)/shard_map/ppermute | solution.py:21
  57.6 1.3 %collective-permute-done.21.refs_13_ = f32[64,768]{1,0:T(8,128)S(1)} collective-permute-done((f32[64,768]{1,0:T(8,128)S(1)}, f32[64,768]{1,0:T(8,128)S(1)}, u32[]{:S(2)}, u32[]{:S(2)}) %collective-permute-start.21) | collective-permute-done | bytes 196640 | tf_op jit(solution)/shard_map/ppermute | solution.py:21
  58.9 1.4 %collective-permute-start.16 = (f32[64,768]{1,0:T(8,128)S(1)}, f32[64,768]{1,0:T(8,128)S(1)}, u32[]{:S(2)}, u32[]{:S(2)}) collective-permute-start(f32[64,768]{1,0:T(8,128)S(1)} %slice.12.refs_4_), channel_id=1, source_target_pairs={{0,4},{2,6},{4,0},{6,2},{1,5},{3,7},{5,1},{7,3},{8,12},{10,14},{12... | collective-permute-start | bytes 589832 | tf_op jit(solution)/shard_map/ppermute | solution.py:21
  60.3 3.6 %collective-permute-done.20.refs_11_ = f32[64,768]{1,0:T(8,128)S(1)} collective-permute-done((f32[64,768]{1,0:T(8,128)S(1)}, f32[64,768]{1,0:T(8,128)S(1)}, u32[]{:S(2)}, u32[]{:S(2)}) %collective-permute-start.20) | collective-permute-done | bytes 196640 | tf_op jit(solution)/shard_map/ppermute | solution.py:21
  63.9 0.7 collective-permute-start.15
  64.6 0.0 copy-done
  64.6 0.0 copy-done.1
  64.6 1.0 %shard_map.190 = (f32[1024,256]{1,0:T(8,128)S(1)}, f32[1024,512]{1,0:T(8,128)S(1)}) custom-call(f32[128,768]{1,0:T(8,128)S(1)} %get-tuple-element.38.whole, bf16[1024,128]{1,0:T(8,128)(2,1)S(1)} %copy-done, bf16[1024,128]{1,0:T(8,128)(2,1)S(1)} %copy-done.1), custom_call_target="tpu_custom_call" | custom-call | tf_op jit(solution)/shard_map/pallas_call | solution.py:215
  65.6 0.0 collective-permute-done.19.refs_10_
  65.6 1.8 %collective-permute-done.18.refs_9_ = f32[64,768]{1,0:T(8,128)S(1)} collective-permute-done((f32[64,768]{1,0:T(8,128)S(1)}, f32[64,768]{1,0:T(8,128)S(1)}, u32[]{:S(2)}, u32[]{:S(2)}) %collective-permute-start.18) | collective-permute-done | bytes 196640 | tf_op jit(solution)/shard_map/ppermute | solution.py:21
  67.4 5.0 %collective-permute-done.17.refs_7_ = f32[64,768]{1,0:T(8,128)S(1)} collective-permute-done((f32[64,768]{1,0:T(8,128)S(1)}, f32[64,768]{1,0:T(8,128)S(1)}, u32[]{:S(2)}, u32[]{:S(2)}) %collective-permute-start.17) | collective-permute-done | bytes 196640 | tf_op jit(solution)/shard_map/ppermute | solution.py:21
  72.3 0.0 collective-permute-done.16.refs_6_
  72.3 2.1 %collective-permute-done.15.refs_5_ = f32[64,768]{1,0:T(8,128)S(1)} collective-permute-done((f32[64,768]{1,0:T(8,128)S(1)}, f32[64,768]{1,0:T(8,128)S(1)}, u32[]{:S(2)}, u32[]{:S(2)}) %collective-permute-start.15) | collective-permute-done | bytes 196640 | tf_op jit(solution)/shard_map/ppermute | solution.py:21
  74.4 2.2 %shard_map.191 = (f32[64,256]{1,0:T(8,128)}, f32[64,512]{1,0:T(8,128)}, f32[64,256]{1,0:T(8,128)}, f32[64,512]{1,0:T(8,128)}, bf16[1024,256]{1,0:T(8,128)(2,1)}, /*index=5*/bf16[1024,512]{1,0:T(8,128)(2,1)}) custom-call(s32[2]{0:T(128)S(1)} %pad_add_fusion.place, f32[2,128]{1,0:T(2,128)S(1)} %add.19.sums, f32[1024,256]{1,0:T(8,128)S(1)} %get-tuple-element.39.query_product, ...), custom_call_target="tpu_custom_call" | custom-call | tf_op jit(solution)/shard_map/pallas_call | solution.py:215
  (6 shorter events, 0.1 us)
Async XLA Ops:
  3.2 61.4 %copy-start = (bf16[1024,128]{1,0:T(8,128)(2,1)S(1)}, bf16[1024,128]{1,0:T(8,128)(2,1)}, u32[]{:S(2)}) copy-start(bf16[1024,128]{1,0:T(8,128)(2,1)} %query_basis.1) | copy-start | bytes 786436
  3.2 61.3 %copy-start.1 = (bf16[1024,128]{1,0:T(8,128)(2,1)S(1)}, bf16[1024,128]{1,0:T(8,128)(2,1)}, u32[]{:S(2)}) copy-start(bf16[1024,128]{1,0:T(8,128)(2,1)} %value_basis.1) | copy-start | bytes 786436
  3.3 9.8 %collective-permute-start = (f32[32,768]{1,0:T(8,128)S(1)}, f32[32,768]{1,0:T(8,128)S(1)}, u32[]{:S(2)}, u32[]{:S(2)}) collective-permute-start(f32[32,768]{1,0:T(8,128)S(1)} %get-tuple-element.32), channel_id=1, source_target_pairs={{0,2},{2,0},{4,6},{6,4},{1,3},{3,1},{5,7},{7,5},{8,10},{10,8},{12,... | collective-permute-start | bytes 294920 | tf_op jit(solution)/shard_map/ppermute | solution.py:21
  6.3 7.4 %collective-permute-start.1 = (f32[32,768]{1,0:T(8,128)S(1)}, f32[32,768]{1,0:T(8,128)S(1)}, u32[]{:S(2)}, u32[]{:S(2)}) collective-permute-start(f32[32,768]{1,0:T(8,128)S(1)} %get-tuple-element.33), channel_id=1, source_target_pairs={{0,4},{2,6},{4,0},{6,2},{1,5},{3,7},{5,1},{7,3},{8,12},{10,14},{12... | collective-permute-start | bytes 294920 | tf_op jit(solution)/shard_map/ppermute | solution.py:21
  7.8 5.9 %collective-permute-start.2 = (f32[32,768]{1,0:T(8,128)S(1)}, f32[32,768]{1,0:T(8,128)S(1)}, u32[]{:S(2)}, u32[]{:S(2)}) collective-permute-start(f32[32,768]{1,0:T(8,128)S(1)} %get-tuple-element.34), channel_id=1, source_target_pairs={{0,6},{2,4},{4,2},{6,0},{1,7},{3,5},{5,3},{7,1},{8,14},{10,12},{12... | collective-permute-start | bytes 294920 | tf_op jit(solution)/shard_map/ppermute | solution.py:21
  9.0 22.6 %collective-permute-start.7 = (f32[80,768]{1,0:T(8,128)S(1)}, f32[80,768]{1,0:T(8,128)S(1)}, u32[]{:S(2)}, u32[]{:S(2)}) collective-permute-start(f32[80,768]{1,0:T(8,128)S(1)} %get-tuple-element.35.refs_0_), channel_id=1, source_target_pairs={{0,24},{8,16},{16,8},{24,0},{1,25},{9,17},{17,9},{25,1},{2,26},{10... | collective-permute-start | bytes 737288 | tf_op jit(solution)/shard_map/ppermute | solution.py:21
  13.1 22.1 %collective-permute-start.6 = (f32[80,768]{1,0:T(8,128)S(1)}, f32[80,768]{1,0:T(8,128)S(1)}, u32[]{:S(2)}, u32[]{:S(2)}) collective-permute-start(f32[80,768]{1,0:T(8,128)S(1)} %get-tuple-element.35.refs_0_), channel_id=1, source_target_pairs={{0,16},{8,24},{16,0},{24,8},{1,17},{9,25},{17,1},{25,9},{2,18},{10... | collective-permute-start | bytes 737288 | tf_op jit(solution)/shard_map/ppermute | solution.py:21
  13.1 22.1 %collective-permute-start.5 = (f32[80,768]{1,0:T(8,128)S(1)}, f32[80,768]{1,0:T(8,128)S(1)}, u32[]{:S(2)}, u32[]{:S(2)}) collective-permute-start(f32[80,768]{1,0:T(8,128)S(1)} %get-tuple-element.35.refs_0_), channel_id=1, source_target_pairs={{0,8},{8,0},{16,24},{24,16},{1,9},{9,1},{17,25},{25,17},{2,10},{10... | collective-permute-start | bytes 737288 | tf_op jit(solution)/shard_map/ppermute | solution.py:21
  13.8 16.4 %collective-permute-start.3 = (f32[32,768]{1,0:T(8,128)S(1)}, f32[32,768]{1,0:T(8,128)S(1)}, u32[]{:S(2)}, u32[]{:S(2)}) collective-permute-start(f32[32,768]{1,0:T(8,128)S(1)} %add_add_fusion), channel_id=1, source_target_pairs={{0,8},{8,0},{16,24},{24,16},{1,9},{9,1},{17,25},{25,17},{2,10},{10... | collective-permute-start | bytes 294920 | tf_op jit(solution)/shard_map/ppermute | solution.py:21
  15.2 25.8 %collective-permute-start.14 = (f32[64,768]{1,0:T(8,128)S(1)}, f32[64,768]{1,0:T(8,128)S(1)}, u32[]{:S(2)}, u32[]{:S(2)}) collective-permute-start(f32[64,768]{1,0:T(8,128)S(1)} %get-tuple-element.41.refs_0_), channel_id=1, source_target_pairs={{0,6},{2,4},{4,2},{6,0},{1,7},{3,5},{5,3},{7,1},{8,14},{10,12},{12... | collective-permute-start | bytes 589832 | tf_op jit(solution)/shard_map/ppermute | solution.py:21
  30.2 6.1 %collective-permute-start.4 = (f32[32,768]{1,0:T(8,128)S(1)}, f32[32,768]{1,0:T(8,128)S(1)}, u32[]{:S(2)}, u32[]{:S(2)}) collective-permute-start(f32[32,768]{1,0:T(8,128)S(1)} %add.18.mine), channel_id=1, source_target_pairs={{0,16},{8,24},{16,0},{24,8},{1,17},{9,25},{17,1},{25,9},{2,18},{10... | collective-permute-start | bytes 294920 | tf_op jit(solution)/shard_map/ppermute | solution.py:21
  31.6 10.9 %collective-permute-start.13 = (f32[64,768]{1,0:T(8,128)S(1)}, f32[64,768]{1,0:T(8,128)S(1)}, u32[]{:S(2)}, u32[]{:S(2)}) collective-permute-start(f32[64,768]{1,0:T(8,128)S(1)} %get-tuple-element.41.refs_0_), channel_id=1, source_target_pairs={{0,4},{2,6},{4,0},{6,2},{1,5},{3,7},{5,1},{7,3},{8,12},{10,14},{12... | collective-permute-start | bytes 589832 | tf_op jit(solution)/shard_map/ppermute | solution.py:21
  37.5 6.6 %collective-permute-start.10 = (f32[32,768]{1,0:T(8,128)S(1)}, f32[32,768]{1,0:T(8,128)S(1)}, u32[]{:S(2)}, u32[]{:S(2)}) collective-permute-start(f32[32,768]{1,0:T(8,128)S(1)} %get-tuple-element.36.refs_0_), channel_id=1, source_target_pairs={{0,6},{2,4},{4,2},{6,0},{1,7},{3,5},{5,3},{7,1},{8,14},{10,12},{12... | collective-permute-start | bytes 294920 | tf_op jit(solution)/shard_map/ppermute | solution.py:21
  39.9 5.6 %collective-permute-start.9 = (f32[32,768]{1,0:T(8,128)S(1)}, f32[32,768]{1,0:T(8,128)S(1)}, u32[]{:S(2)}, u32[]{:S(2)}) collective-permute-start(f32[32,768]{1,0:T(8,128)S(1)} %get-tuple-element.36.refs_0_), channel_id=1, source_target_pairs={{0,4},{2,6},{4,0},{6,2},{1,5},{3,7},{5,1},{7,3},{8,12},{10,14},{12... | collective-permute-start | bytes 294920 | tf_op jit(solution)/shard_map/ppermute | solution.py:21
  40.4 6.6 %collective-permute-start.8 = (f32[32,768]{1,0:T(8,128)S(1)}, f32[32,768]{1,0:T(8,128)S(1)}, u32[]{:S(2)}, u32[]{:S(2)}) collective-permute-start(f32[32,768]{1,0:T(8,128)S(1)} %get-tuple-element.36.refs_0_), channel_id=1, source_target_pairs={{0,2},{2,0},{4,6},{6,4},{1,3},{3,1},{5,7},{7,5},{8,10},{10,8},{12,... | collective-permute-start | bytes 294920 | tf_op jit(solution)/shard_map/ppermute | solution.py:21
  41.0 9.4 %collective-permute-start.12 = (f32[64,768]{1,0:T(8,128)S(1)}, f32[64,768]{1,0:T(8,128)S(1)}, u32[]{:S(2)}, u32[]{:S(2)}) collective-permute-start(f32[64,768]{1,0:T(8,128)S(1)} %get-tuple-element.41.refs_0_), channel_id=1, source_target_pairs={{0,2},{2,0},{4,6},{6,4},{1,3},{3,1},{5,7},{7,5},{8,10},{10,8},{12,... | collective-permute-start | bytes 589832 | tf_op jit(solution)/shard_map/ppermute | solution.py:21
  42.5 13.0 %collective-permute-start.23 = (f32[64,768]{1,0:T(8,128)S(1)}, f32[64,768]{1,0:T(8,128)S(1)}, u32[]{:S(2)}, u32[]{:S(2)}) collective-permute-start(f32[64,768]{1,0:T(8,128)S(1)} %slice.14.refs_12_), channel_id=1, source_target_pairs={{0,6},{2,4},{4,2},{6,0},{1,7},{3,5},{5,3},{7,1},{8,14},{10,12},{12... | collective-permute-start | bytes 589832 | tf_op jit(solution)/shard_map/ppermute | solution.py:21
  44.1 12.0 %collective-permute-start.22 = (f32[64,768]{1,0:T(8,128)S(1)}, f32[64,768]{1,0:T(8,128)S(1)}, u32[]{:S(2)}, u32[]{:S(2)}) collective-permute-start(f32[64,768]{1,0:T(8,128)S(1)} %slice.14.refs_12_), channel_id=1, source_target_pairs={{0,4},{2,6},{4,0},{6,2},{1,5},{3,7},{5,1},{7,3},{8,12},{10,14},{12... | collective-permute-start | bytes 589832 | tf_op jit(solution)/shard_map/ppermute | solution.py:21
  45.6 13.3 %collective-permute-start.21 = (f32[64,768]{1,0:T(8,128)S(1)}, f32[64,768]{1,0:T(8,128)S(1)}, u32[]{:S(2)}, u32[]{:S(2)}) collective-permute-start(f32[64,768]{1,0:T(8,128)S(1)} %slice.14.refs_12_), channel_id=1, source_target_pairs={{0,2},{2,0},{4,6},{6,4},{1,3},{3,1},{5,7},{7,5},{8,10},{10,8},{12,... | collective-permute-start | bytes 589832 | tf_op jit(solution)/shard_map/ppermute | solution.py:21
  47.1 16.8 %collective-permute-start.20 = (f32[64,768]{1,0:T(8,128)S(1)}, f32[64,768]{1,0:T(8,128)S(1)}, u32[]{:S(2)}, u32[]{:S(2)}) collective-permute-start(f32[64,768]{1,0:T(8,128)S(1)} %slice.13.refs_8_), channel_id=1, source_target_pairs={{0,6},{2,4},{4,2},{6,0},{1,7},{3,5},{5,3},{7,1},{8,14},{10,12},{12... | collective-permute-start | bytes 589832 | tf_op jit(solution)/shard_map/ppermute | solution.py:21
  50.4 1.2 %collective-permute-start.11 = (f32[2,128]{1,0:T(2,128)S(1)}, f32[2,128]{1,0:T(2,128)S(1)}, u32[]{:S(2)}, u32[]{:S(2)}) collective-permute-start(f32[2,128]{1,0:T(2,128)S(1)} %get-tuple-element.37), channel_id=1, source_target_pairs={{0,1},{1,0},{2,3},{3,2},{4,5},{5,4},{6,7},{7,6},{8,9},{9,8},{10,11... | collective-permute-start | bytes 3080 | tf_op jit(solution)/shard_map/ppermute | solution.py:21
  51.6 14.0 %collective-permute-start.19 = (f32[64,768]{1,0:T(8,128)S(1)}, f32[64,768]{1,0:T(8,128)S(1)}, u32[]{:S(2)}, u32[]{:S(2)}) collective-permute-start(f32[64,768]{1,0:T(8,128)S(1)} %slice.13.refs_8_), channel_id=1, source_target_pairs={{0,4},{2,6},{4,0},{6,2},{1,5},{3,7},{5,1},{7,3},{8,12},{10,14},{12... | collective-permute-start | bytes 589832 | tf_op jit(solution)/shard_map/ppermute | solution.py:21
  55.5 11.9 %collective-permute-start.18 = (f32[64,768]{1,0:T(8,128)S(1)}, f32[64,768]{1,0:T(8,128)S(1)}, u32[]{:S(2)}, u32[]{:S(2)}) collective-permute-start(f32[64,768]{1,0:T(8,128)S(1)} %slice.13.refs_8_), channel_id=1, source_target_pairs={{0,2},{2,0},{4,6},{6,4},{1,3},{3,1},{5,7},{7,5},{8,10},{10,8},{12,... | collective-permute-start | bytes 589832 | tf_op jit(solution)/shard_map/ppermute | solution.py:21
  56.1 16.2 %collective-permute-start.17 = (f32[64,768]{1,0:T(8,128)S(1)}, f32[64,768]{1,0:T(8,128)S(1)}, u32[]{:S(2)}, u32[]{:S(2)}) collective-permute-start(f32[64,768]{1,0:T(8,128)S(1)} %slice.12.refs_4_), channel_id=1, source_target_pairs={{0,6},{2,4},{4,2},{6,0},{1,7},{3,5},{5,3},{7,1},{8,14},{10,12},{12... | collective-permute-start | bytes 589832 | tf_op jit(solution)/shard_map/ppermute | solution.py:21
  58.9 13.5 %collective-permute-start.16 = (f32[64,768]{1,0:T(8,128)S(1)}, f32[64,768]{1,0:T(8,128)S(1)}, u32[]{:S(2)}, u32[]{:S(2)}) collective-permute-start(f32[64,768]{1,0:T(8,128)S(1)} %slice.12.refs_4_), channel_id=1, source_target_pairs={{0,4},{2,6},{4,0},{6,2},{1,5},{3,7},{5,1},{7,3},{8,12},{10,14},{12... | collective-permute-start | bytes 589832 | tf_op jit(solution)/shard_map/ppermute | solution.py:21
  63.9 10.5 %collective-permute-start.15 = (f32[64,768]{1,0:T(8,128)S(1)}, f32[64,768]{1,0:T(8,128)S(1)}, u32[]{:S(2)}, u32[]{:S(2)}) collective-permute-start(f32[64,768]{1,0:T(8,128)S(1)} %slice.12.refs_4_), channel_id=1, source_target_pairs={{0,2},{2,0},{4,6},{6,4},{1,3},{3,1},{5,7},{7,5},{8,10},{10,8},{12,... | collective-permute-start | bytes 589832 | tf_op jit(solution)/shard_map/ppermute | solution.py:21
where the time goes:
time: 76.7 us; the launch traced here: 76.6 us
  waiting for transfers between devices  35 us (46%)
  starting transfers between devices  32 us (42%)
  Pallas kernels  8.64 us (11%)
  between operations  0.77 us (1%)
    ppermute x24, waiting for transfers between devices, swap(): return lax.ppermute(block, axis, pairs)  35 us
    ppermute x24, starting transfers between devices, swap(): return lax.ppermute(block, axis, pairs)  32 us
    pallas_call x6, Pallas kernels, call(): pl.pallas_call(kernel, out_shape=out_shape, in_specs=specs, out_specs=jax...  8.64 us
  transfers between devices with their start and end apart: 24, of which 11 were waited for; matrix products, arithmetic and copies ran while one was open for 0% of the time, Pallas kernels for 5%

commit v1 on v0

--- a/solution.py
+++ b/solution.py
@@ -56,42 +56,32 @@
     return pl.ds(pl.multiple_of(start * size, size), size)
 
 
-def stage_kernel(query_weight, value_weight, query_first, value_first, *refs):
-    query_second, value_second, weights, own, sems = refs
+def stage_kernel(*refs):
+    query_weight, value_weight, query_first, value_first, query_second, value_second = refs[:6]
+    sources, weights, own, targets, sems = refs[6:11], refs[11], refs[12], refs[13:18], refs[18]
     rows, ranks = query_weight.shape[0], query_first.shape[0]
     query_width, width = query_weight.shape[1], weights.shape[1]
-    copies = []
+    jobs = []
     for target, left, right, low in (
         (weights, query_weight, value_weight, 0),
         (own, query_weight, value_weight, 0),
         (own, query_first, value_first, rows),
         (own, query_second, value_second, rows + ranks),
     ):
-        for source, columns in ((left, pl.ds(0, query_width)), (right, pl.ds(query_width, width - query_width))):
-            copies.append(
-                pltpu.make_async_copy(
-                    source, target.at[pl.ds(low, source.shape[0]), columns], sems.at[len(copies)]
-                )
-            )
+        where = pl.ds(low, left.shape[0])
+        jobs.append((left, target.at[where, pl.ds(0, query_width)]))
+        jobs.append((right, target.at[where, pl.ds(query_width, width - query_width)]))
+    jobs.extend(zip(sources, targets))
+    copies = [pltpu.make_async_copy(*job, sems.at[i]) for i, job in enumerate(jobs)]
     for copy in copies:
         copy.start()
     for copy in copies:
         copy.wait()
 
 
-def project_kernel(counts, place, *refs):
+def project_kernel(counts, place, tokens, query_basis, value_basis, query_cot, value_cot, *refs):
     fs, rep, ranks = counts
-    sources, chunks, total = refs[:5], refs[5 : 5 + rep], refs[5 + rep]
-    tokens, query_basis, value_basis, query_cot, value_cot = held = refs[6 + rep : 11 + rep]
-    sems = refs[11 + rep]
-    copies = [
-        pltpu.make_async_copy(source, target, sems.at[i])
-        for i, (source, target) in enumerate(zip(sources, held))
-    ]
-    for copy in copies:
-        copy.start()
-    for copy in copies:
-        copy.wait()
+    chunks, total = refs[:rep], refs[rep]
     r = place[1]
     query_width = query_cot.shape[1]
     for basis, cot, lo in ((query_basis, query_cot, 0), (value_basis, value_cot, query_width)):
@@ -106,23 +96,32 @@
             ]
 
 
-def moments_kernel(counts, place, mine, other, *refs):
-    fs, rows, ranks, query_width = counts
-    blocks, (query_first, query_second, value_first, value_second, direction) = refs[:fs], refs[fs:]
+def direction_kernel(counts, place, mine, other, *refs):
+    fs, rows, ranks = counts
+    blocks, direction = refs[:fs], refs[fs]
     z = place[0]
     for k in range(fs):
         where = aligned(z ^ k, ranks)
-        first, second, ratio = moments(
+        direction[where, :] = moments(
             mine[where, :] + other[where, :],
             blocks[k][rows : rows + ranks, :],
             blocks[k][rows + ranks : rows + 2 * ranks, :],
-        )
-        direction[where, :] = ratio
-        if k == 0:
-            query_first[...] = first[:, :query_width]
-            query_second[...] = second[:, :query_width]
-            value_first[...] = first[:, query_width:]
-            value_second[...] = second[:, query_width:]
+        )[2]
+
+
+def record_kernel(counts, place, mine, other, own, *refs):
+    rows, ranks, query_width = counts
+    query_first, query_second, value_first, value_second = refs
+    where = aligned(place[0], ranks)
+    first, second, _ = moments(
+        mine[where, :] + other[where, :],
+        own[rows : rows + ranks, :],
+        own[rows + ranks : rows + 2 * ranks, :],
+    )
+    query_first[...] = first[:, :query_width]
+    query_second[...] = second[:, :query_width]
+    value_first[...] = first[:, query_width:]
+    value_second[...] = second[:, query_width:]
 
 
 def whole_kernel(counts, place, *refs):
@@ -158,28 +157,48 @@
         )
 
 
-def finish_kernel(counts, place, sums, query_product, value_product, *refs):
-    fs, rep, rows, entries = counts
-    blocks = refs[: fs * rep]
-    query_update, value_update, query_new, value_new, query_copy, value_copy = refs[fs * rep :]
+def finish_kernel(counts, pieces, place, sums, query_product, value_product, *refs):
+    rep, rows, entries, blocks = counts
+    sources, refs = refs[:blocks], refs[blocks:]
     z, r = place[0], place[1]
     query_width = query_product.shape[1]
     query_scale = 1.0 / jnp.sqrt(sums[0:1, 0:1] / entries[0] + 1.0)
     value_scale = 1.0 / jnp.sqrt(sums[1:2, 0:1] / entries[1] + 1.0)
-    for kz in range(fs):
-        for kr in range(rep):
-            where = aligned((z ^ kz) * rep + (r ^ kr), rows)
-            held = blocks[kz * rep + kr]
-            for product, scale, lo, update, new, copy in (
-                (query_product, query_scale, 0, query_update, query_new, query_copy),
-                (value_product, value_scale, query_width, value_update, value_new, value_copy),
-            ):
-                step = product[where, :] * scale
-                weight = held[:, lo : lo + product.shape[1]] - 0.01 * step
-                copy[where, :] = weight.astype(BF16)
-                if kz == 0 and kr == 0:
-                    update[...] = step
-                    new[...] = weight
+    own = any(kz == 0 and kr == 0 for kz, kr, *_ in pieces)
+    if own:
+        query_update, value_update, query_new, value_new, query_copy, value_copy = refs[:6]
+        updates, news = (query_update, value_update), (query_new, value_new)
+        refs = refs[6:]
+    else:
+        query_copy, value_copy = refs[2:4]
+        refs = refs[4:]
+    query_held, value_held, sems = refs
+    copies = []
+    filled = 0
+    for kz, kr, source, start, offset, size in pieces:
+        owner = (z ^ kz) * rep + (r ^ kr)
+        where = pl.ds(pl.multiple_of(owner * rows + offset, size), size)
+        slot = pl.ds(filled, size)
+        for i, (product, scale, lo, held, copy) in enumerate(
+            (
+                (query_product, query_scale, 0, query_held, query_copy),
+                (value_product, value_scale, query_width, value_held, value_copy),
+            )
+        ):
+            step = product[where, :] * scale
+            old = sources[source][start : start + size, lo : lo + product.shape[1]]
+            weight = old - 0.01 * step
+            held[slot, :] = weight.astype(BF16)
+            if kz == 0 and kr == 0:
+                updates[i][...] = step
+                news[i][...] = weight
+            copies.append(
+                pltpu.make_async_copy(held.at[slot, :], copy.at[where, :], sems.at[len(copies)])
+            )
+            copies[-1].start()
+        filled += size
+    for copy in copies:
+        copy.wait()
 
 
 def kernel_body(
@@ -205,7 +224,7 @@
     def shape(*dims, dtype=F32):
         return jax.ShapeDtypeStruct(dims, dtype)
 
-    def call(kernel, out_shape, *operands, scratch=(), outside=()):
+    def call(kernel, out_shape, *operands, scratch=(), outside=(), outside_out=(), aliases=None):
         specs = [SMEM if operand is place else VMEM for operand in operands]
         specs = [ANY if i in outside else spec for i, spec in enumerate(specs)]
         operands = [
@@ -216,43 +235,62 @@
             kernel,
             out_shape=out_shape,
             in_specs=specs,
-            out_specs=jax.tree.map(lambda _: VMEM, out_shape),
+            out_specs=tuple(ANY if i in outside_out else VMEM for i in range(len(out_shape))),
             scratch_shapes=scratch,
+            input_output_aliases=aliases or {},
             compiler_params=PARAMS,
         )(*operands)
 
-    weights, own = call(
+    operands = (normed_input, query_basis, value_basis, query_cotangent, value_cotangent)
+    weights, own, *staged = call(
         stage_kernel,
-        (shape(rows, width), shape(rows + 2 * ranks, width)),
+        (shape(rows, width), shape(rows + 2 * ranks, width))
+        + tuple(shape(*operand.shape, dtype=operand.dtype) for operand in operands),
         query_weight,
         value_weight,
         query_first,
         value_first,
         query_second,
         value_second,
-        scratch=[pltpu.SemaphoreType.DMA((8,))],
-        outside=range(6),
-    )
-    plane = spread(weights, "rep")
-    along = spread(own, "fs")
-
-    operands = (normed_input, query_basis, value_basis, query_cotangent, value_cotangent)
+        *operands,
+        scratch=[pltpu.SemaphoreType.DMA((13,))],
+        outside=range(11),
+    )
+    query_basis, value_basis = staged[1:3]
+    half = rows // 2
+
+    def sides(block, extra=None):
+        payloads = [block, block]
+        if extra is not None:
+            payloads = [
+                jnp.concatenate([block, extra[1][half:rows]], axis=0),
+                jnp.concatenate([block, extra[0][:half]], axis=0),
+            ]
+        return [swap(payloads[k - 1], "rep", k) for k in (1, 2)]
+
+    plane = sides(weights)
+    along = [own]
+    for k in range(1, fs):
+        source, mask = (along[k - 1], 1) if k % 2 and k > 1 else (own, k)
+        along.append(swap(source, "fs", mask))
     chunks = call(
         functools.partial(project_kernel, (fs, rep, ranks)),
         (shape(fs * ranks, width),) * rep,
         place,
-        *operands,
-        scratch=[pltpu.VMEM((fs * rep * ranks, width), F32)]
-        + [pltpu.VMEM(operand.shape, operand.dtype) for operand in operands]
-        + [pltpu.SemaphoreType.DMA((5,))],
-        outside=range(1, 6),
+        *staged,
+        scratch=[pltpu.VMEM((fs * rep * ranks, width), F32)],
     )
     arrived = [swap(chunks[k], "rep", k) for k in range(1, rep)]
     mine = functools.reduce(jnp.add, arrived, chunks[0])
-    far = []
+    far = [plane]
     for k in range(1, fs):
         cut = along[k][:rows]
-        far.append(spread(cut, "rep"))
+        blocks = sides(cut, plane if k == 1 else None)
+        if k == fs - 1:
+            blocks.append(swap(cut, "rep", 3))
+        far.append(blocks)
+    cross = jnp.concatenate([far[1][1][rows:], far[1][0][rows:]], axis=0)
+    crosses = [swap(cross, "fs", k) for k in range(1, fs - 1)]
     step = 1
     while 2 * step < fs:
         arrived = swap(mine, "fs", step)
@@ -260,21 +298,28 @@
         step *= 2
     other = swap(mine, "fs", step)
 
-    *new_moments, direction = call(
-        functools.partial(moments_kernel, (fs, rows, ranks, query_width)),
-        (shape(ranks, query_width),) * 2
-        + (shape(ranks, value_width),) * 2
-        + (shape(fs * ranks, width),),
+    (direction,) = call(
+        functools.partial(direction_kernel, (fs, rows, ranks)),
+        (shape(fs * ranks, width),),
         place,
         mine,
         other,
         *along,
     )
+    wholes = spread(direction, "rep")
+    new_moments = call(
+        functools.partial(record_kernel, (rows, ranks, query_width)),
+        (shape(ranks, query_width),) * 2 + (shape(ranks, value_width),) * 2,
+        place,
+        mine,
+        other,
+        own,
+    )
     whole, sums = call(
         functools.partial(whole_kernel, (fs, rep, ranks, query_width)),
         (shape(fs * rep * ranks, width), shape(2, 128)),
         place,
-        *spread(direction, "rep"),
+        *wholes,
     )
     if tp == 2:
         sums = sums + swap(sums, "tp", 1)
@@ -287,17 +332,56 @@
         query_basis,
         value_basis,
     )
-    held = plane + sum(far, [])
+
     entries = (fs * rep * ranks * query_width * tp, fs * rep * ranks * value_width * tp)
-    query_update, value_update, query_new, value_new, query_copy, value_copy = call(
-        functools.partial(finish_kernel, (fs, rep, rows, entries)),
-        (shape(rows, query_width), shape(rows, value_width)) * 2
-        + (shape(total, query_width, dtype=BF16), shape(total, value_width, dtype=BF16)),
-        place,
-        sums,
-        *products,
-        *held,
-    )
+    copy_shapes = (shape(total, query_width, dtype=BF16), shape(total, value_width, dtype=BF16))
+
+    def finish(pieces, copies=None):
+        sources = []
+        for piece in pieces:
+            if not any(piece[2] is source for source in sources):
+                sources.append(piece[2])
+        found = [[i for i, s in enumerate(sources) if s is piece[2]][0] for piece in pieces]
+        pieces = [(p[0], p[1], i, *p[3:]) for p, i in zip(pieces, found)]
+        held = sum(piece[-1] for piece in pieces)
+        first = 4 + len(sources)
+        kernel = functools.partial(finish_kernel, (rep, rows, entries, len(sources)), pieces)
+        scratch = [
+            pltpu.VMEM((held, query_width), BF16),
+            pltpu.VMEM((held, value_width), BF16),
+            pltpu.SemaphoreType.DMA((2 * len(pieces),)),
+        ]
+        if copies is None:
+            shapes = (shape(rows, query_width), shape(rows, value_width)) * 2 + copy_shapes
+            return call(
+                kernel, shapes, place, sums, *products, *sources, scratch=scratch, outside_out=(4, 5)
+            )
+        return call(
+            kernel,
+            copy_shapes,
+            place,
+            sums,
+            *products,
+            *sources,
+            *copies,
+            scratch=scratch,
+            outside=(first, first + 1),
+            outside_out=(0, 1),
+            aliases={first: 0, first + 1: 1},
+        )
+
+    early, late = [], []
+    for kz in range(fs):
+        group = late if kz == fs - 1 else early
+        early.append((kz, 0, along[kz], 0, 0, rows))
+        for kr in (1, 2):
+            group.append((kz, kr, far[kz][kr - 1], 0, 0, rows))
+        if kz == fs - 1:
+            late.append((kz, 3, far[kz][2], 0, 0, rows))
+        else:
+            (late if kz == fs - 2 else early).append((kz, 3, ([cross] + crosses)[kz], 0, 0, rows))
+    query_update, value_update, query_new, value_new, *copies = finish(early)
+    query_copy, value_copy = finish(late, copies)
     query_first_new, query_second_new, value_first_new, value_second_new = new_moments
     return (
         query_update,
@@ -387,7 +471,7 @@
     query_weight, value_weight, query_first = operands[5:8]
     fits = query_first.shape[0] % 8 == 0 and query_weight.shape[0] % 16 == 0
     fits = fits and query_weight.shape[1] % 128 == 0 and value_weight.shape[1] % 128 == 0
-    if fits and lax.axis_size("fs") >= 4:
+    if fits and lax.axis_size("fs") >= 4 and lax.axis_size("rep") == 4:
         return kernel_body(*operands)
     return plain_body(*operands)
 

time: 76.7 us -> 61.5 us (0.80)
  waiting for transfers between devices: 35 us -> 20 us
  starting transfers between devices: 32 us -> 30 us
  Pallas kernels: 8.64 us -> 10.3 us
    ppermute x24 -> x23, waiting for transfers between devices: 35 us -> 20 us  [swap(): return lax.ppermute(block, axis, pairs)]
    ppermute x24 -> x23, starting transfers between devices: 32 us -> 30 us  [swap(): return lax.ppermute(block, axis, pairs)]
    pallas_call x6 -> x8, Pallas kernels: 8.64 us -> 10.3 us  [call(): pl.pallas_call(kernel, out_shape=out_shape, in_specs=specs, out_specs=tup...]
  transfers between devices with their start and end apart: 24 -> 23, of which waited for: 11 -> 9; matrix products, arithmetic and copies ran while one was open for 0% -> 0% of each run, Pallas kernels for 5% -> 12%
where the time goes in v1:
time: 61.5 us; the launch traced here: 61.4 us
  starting transfers between devices  30 us (49%)
  waiting for transfers between devices  20 us (33%)
  Pallas kernels  10.3 us (17%)
  between operations  0.83 us (1%)
    ppermute x23, starting transfers between devices, swap(): return lax.ppermute(block, axis, pairs)  30 us
    ppermute x23, waiting for transfers between devices, swap(): return lax.ppermute(block, axis, pairs)  20 us
    pallas_call x8, Pallas kernels, call(): pl.pallas_call(kernel, out_shape=out_shape, in_specs=specs, out_specs=tup...  10.3 us
  transfers between devices with their start and end apart: 23, of which 9 were waited for; matrix products, arithmetic and copies ran while one was open for 0% of the time, Pallas kernels for 12%

profile of v1, /device:TPU:0, one launch (start us, length us, event | category | flops | bytes accessed | tf_op | source)
XLA Modules:
  0.0 61.4 jit_solution(10157068186476592018)
XLA Ops:
  0.6 1.5 %shard_map.186 = (f32[64,768]{1,0:T(8,128)S(1)}, f32[80,768]{1,0:T(8,128)S(1)}, bf16[128,1024]{1,0:T(8,128)(2,1)S(1)}, bf16[1024,128]{1,0:T(8,128)(2,1)S(1)}, bf...) custom-call(f32[64,256]{1,0:T(8,128)} %refs_0_.1, f32[64,512]{1,0:T(8,128)} %refs_1_.1, ...), custom_call_target="tpu_custom_call" | custom-call | tf_op jit(solution)/shard_map/pallas_call | solution.py:234
  2.2 3.1 %collective-permute-start.5 = (f32[80,768]{1,0:T(8,128)S(1)}, f32[80,768]{1,0:T(8,128)S(1)}, u32[]{:S(2)}, u32[]{:S(2)}) collective-permute-start(f32[80,768]{1,0:T(8,128)S(1)} %get-tuple-element.46.refs_0_.own), channel_id=1, source_target_pairs={{0,8},{8,0},{16,24},{24,16},{1,9},{9,1},{17,25},{25,17},{2,10},{10... | collective-permute-start | bytes 737288 | tf_op jit(solution)/shard_map/ppermute | solution.py:21
  5.3 1.5 %collective-permute-start.12 = (f32[64,768]{1,0:T(8,128)S(1)}, f32[64,768]{1,0:T(8,128)S(1)}, u32[]{:S(2)}, u32[]{:S(2)}) collective-permute-start(f32[64,768]{1,0:T(8,128)S(1)} %get-tuple-element.51), channel_id=1, source_target_pairs={{0,2},{2,0},{4,6},{6,4},{1,3},{3,1},{5,7},{7,5},{8,10},{10,8},{12,... | collective-permute-start | bytes 589832 | tf_op jit(solution)/shard_map/ppermute | solution.py:21
  6.8 1.5 %collective-permute-start.13 = (f32[64,768]{1,0:T(8,128)S(1)}, f32[64,768]{1,0:T(8,128)S(1)}, u32[]{:S(2)}, u32[]{:S(2)}) collective-permute-start(f32[64,768]{1,0:T(8,128)S(1)} %get-tuple-element.51), channel_id=1, source_target_pairs={{0,4},{2,6},{4,0},{6,2},{1,5},{3,7},{5,1},{7,3},{8,12},{10,14},{12... | collective-permute-start | bytes 589832 | tf_op jit(solution)/shard_map/ppermute | solution.py:21
  8.3 2.6 %collective-permute-start.6 = (f32[80,768]{1,0:T(8,128)S(1)}, f32[80,768]{1,0:T(8,128)S(1)}, u32[]{:S(2)}, u32[]{:S(2)}) collective-permute-start(f32[80,768]{1,0:T(8,128)S(1)} %get-tuple-element.46.refs_0_.own), channel_id=1, source_target_pairs={{0,16},{8,24},{16,0},{24,8},{1,17},{9,25},{17,1},{25,9},{2,18},{10... | collective-permute-start | bytes 737288 | tf_op jit(solution)/shard_map/ppermute | solution.py:21
  10.9 0.1 pad_add_fusion.place
  11.0 1.3 %shard_map.187 = (f32[32,768]{1,0:T(8,128)S(1)}, f32[32,768]{1,0:T(8,128)S(1)}, f32[32,768]{1,0:T(8,128)S(1)}, f32[32,768]{1,0:T(8,128)S(1)}) custom-call(s32[2]{0:T(128)S(1)} %pad_add_fusion.place, bf16[128,1024]{1,0:T(8,128)(2,1)S(1)} %get-tuple-element.37.tokens, bf16[1024,128]{1,0:T(8,128)(2,1)S(1)} %get-tuple-element.38.query_basis, ...), custom_call_target="tpu_custom_call" | custom-call | tf_op jit(solution)/shard_map/pallas_call | solution.py:234
  12.3 0.6 collective-permute-start
  12.9 0.0 collective-permute-done.12.refs_1_
  12.9 0.5 collective-permute-start.1
  13.4 0.0 collective-permute-done.13.refs_2_
  13.4 2.5 %collective-permute-start.2 = (f32[32,768]{1,0:T(8,128)S(1)}, f32[32,768]{1,0:T(8,128)S(1)}, u32[]{:S(2)}, u32[]{:S(2)}) collective-permute-start(f32[32,768]{1,0:T(8,128)S(1)} %get-tuple-element.45), channel_id=1, source_target_pairs={{0,6},{2,4},{4,2},{6,0},{1,7},{3,5},{5,3},{7,1},{8,14},{10,12},{12... | collective-permute-start | bytes 294920 | tf_op jit(solution)/shard_map/ppermute | solution.py:21
  15.9 0.0 collective-permute-done.5.refs_1_.refs_4_
  16.0 0.1 pad_maximum_fusion.1
  16.0 0.8 %collective-permute-start.14 = (f32[96,768]{1,0:T(8,128)S(1)}, f32[96,768]{1,0:T(8,128)S(1)}, u32[]{:S(2)}, u32[]{:S(2)}) collective-permute-start(f32[96,768]{1,0:T(8,128)S(1)} %get-tuple-element.64), channel_id=1, source_target_pairs={{0,4},{2,6},{4,0},{6,2},{1,5},{3,7},{5,1},{7,3},{8,12},{10,14},{12... | collective-permute-start | bytes 884744 | tf_op jit(solution)/shard_map/ppermute | solution.py:21
  16.8 0.5 collective-permute-done
  17.3 2.0 %collective-permute-start.15 = (f32[96,768]{1,0:T(8,128)S(1)}, f32[96,768]{1,0:T(8,128)S(1)}, u32[]{:S(2)}, u32[]{:S(2)}) collective-permute-start(f32[96,768]{1,0:T(8,128)S(1)} %get-tuple-element.65), channel_id=1, source_target_pairs={{0,2},{2,0},{4,6},{6,4},{1,3},{3,1},{5,7},{7,5},{8,10},{10,8},{12,... | collective-permute-start | bytes 884744 | tf_op jit(solution)/shard_map/ppermute | solution.py:21
  19.3 2.1 %collective-permute-done.6.refs_2_.refs_8_ = f32[80,768]{1,0:T(8,128)S(1)} collective-permute-done((f32[80,768]{1,0:T(8,128)S(1)}, f32[80,768]{1,0:T(8,128)S(1)}, u32[]{:S(2)}, u32[]{:S(2)}) %collective-permute-start.6) | collective-permute-done | bytes 245792 | tf_op jit(solution)/shard_map/ppermute | solution.py:21
  21.4 0.0 collective-permute-start.7
  21.4 0.0 collective-permute-done.1
  21.4 0.0 collective-permute-done.2
  21.4 2.1 %collective-permute-start.3 = (f32[32,768]{1,0:T(8,128)S(1)}, f32[32,768]{1,0:T(8,128)S(1)}, u32[]{:S(2)}, u32[]{:S(2)}) collective-permute-start(f32[32,768]{1,0:T(8,128)S(1)} %add_add_fusion), channel_id=1, source_target_pairs={{0,8},{8,0},{16,24},{24,16},{1,9},{9,1},{17,25},{25,17},{2,10},{10... | collective-permute-start | bytes 294920 | tf_op jit(solution)/shard_map/ppermute | solution.py:21
  23.5 6.2 %collective-permute-done.3 = f32[32,768]{1,0:T(8,128)S(1)} collective-permute-done((f32[32,768]{1,0:T(8,128)S(1)}, f32[32,768]{1,0:T(8,128)S(1)}, u32[]{:S(2)}, u32[]{:S(2)}) %collective-permute-start.3) | collective-permute-done | bytes 98336 | tf_op jit(solution)/shard_map/ppermute | solution.py:21
  29.8 1.6 %collective-permute-start.4 = (f32[32,768]{1,0:T(8,128)S(1)}, f32[32,768]{1,0:T(8,128)S(1)}, u32[]{:S(2)}, u32[]{:S(2)}) collective-permute-start(f32[32,768]{1,0:T(8,128)S(1)} %add.18.mine), channel_id=1, source_target_pairs={{0,16},{8,24},{16,0},{24,8},{1,17},{9,25},{17,1},{25,9},{2,18},{10... | collective-permute-start | bytes 294920 | tf_op jit(solution)/shard_map/ppermute | solution.py:21
  31.4 4.8 %collective-permute-done.4.other = f32[32,768]{1,0:T(8,128)S(1)} collective-permute-done((f32[32,768]{1,0:T(8,128)S(1)}, f32[32,768]{1,0:T(8,128)S(1)}, u32[]{:S(2)}, u32[]{:S(2)}) %collective-permute-start.4) | collective-permute-done | bytes 98336 | tf_op jit(solution)/shard_map/ppermute | solution.py:21
  36.2 0.0 collective-permute-done.7.refs_3_.refs_11_
  36.2 0.6 %shard_map.188.refs_0_ = f32[32,768]{1,0:T(8,128)S(1)} custom-call(s32[2]{0:T(128)S(1)} %pad_add_fusion.place, f32[32,768]{1,0:T(8,128)S(1)} %add.18.mine, f32[32,768]{1,0:T(8,128)S(1)} %collective-permute-done.4.other, f32[80,768]{1,0:T(8,128)S(1)} %get-tuple-element.46.refs_0_.own, f32[80,768]{1,0:T(8,128)S(1)} %collective-permute-done.5.refs_1_.refs_4_, ...), custom_call_target="tpu_custom_call" | custom-call | tf_op jit(solution)/shard_map/pallas_call | solution.py:234
  36.9 0.1 collective-permute-start.10
  36.9 1.1 %collective-permute-start.8 = (f32[32,768]{1,0:T(8,128)S(1)}, f32[32,768]{1,0:T(8,128)S(1)}, u32[]{:S(2)}, u32[]{:S(2)}) collective-permute-start(f32[32,768]{1,0:T(8,128)S(1)} %shard_map.188.refs_0_), channel_id=1, source_target_pairs={{0,2},{2,0},{4,6},{6,4},{1,3},{3,1},{5,7},{7,5},{8,10},{10,8},{12,... | collective-permute-start | bytes 294920 | tf_op jit(solution)/shard_map/ppermute | solution.py:21
  38.1 2.3 %collective-permute-start.9 = (f32[32,768]{1,0:T(8,128)S(1)}, f32[32,768]{1,0:T(8,128)S(1)}, u32[]{:S(2)}, u32[]{:S(2)}) collective-permute-start(f32[32,768]{1,0:T(8,128)S(1)} %shard_map.188.refs_0_), channel_id=1, source_target_pairs={{0,4},{2,6},{4,0},{6,2},{1,5},{3,7},{5,1},{7,3},{8,12},{10,14},{12... | collective-permute-start | bytes 294920 | tf_op jit(solution)/shard_map/ppermute | solution.py:21
  40.4 0.0 collective-permute-done.14.refs_6_
  40.4 0.1 collective-permute-start.17
  40.5 0.0 collective-permute-done.15.refs_5_
  40.5 0.6 %collective-permute-start.18 = (f32[64,768]{1,0:T(8,128)S(1)}, f32[64,768]{1,0:T(8,128)S(1)}, u32[]{:S(2)}, u32[]{:S(2)}) collective-permute-start(f32[64,768]{1,0:T(8,128)S(1)} %slice.33), channel_id=1, source_target_pairs={{0,4},{2,6},{4,0},{6,2},{1,5},{3,7},{5,1},{7,3},{8,12},{10,14},{12... | collective-permute-start | bytes 589832 | tf_op jit(solution)/shard_map/ppermute | solution.py:21
  41.2 1.3 %collective-permute-done.10.refs_3_ = f32[32,768]{1,0:T(8,128)S(1)} collective-permute-done((f32[32,768]{1,0:T(8,128)S(1)}, f32[32,768]{1,0:T(8,128)S(1)}, u32[]{:S(2)}, u32[]{:S(2)}) %collective-permute-start.10) | collective-permute-done | bytes 98336 | tf_op jit(solution)/shard_map/ppermute | solution.py:21
  42.5 0.6 collective-permute-done.8.refs_1_
  43.1 0.4 collective-permute-done.9.refs_2_
  43.5 0.7 %shard_map.189 = (f32[128,768]{1,0:T(8,128)S(1)}, f32[2,128]{1,0:T(2,128)S(1)}) custom-call(s32[2]{0:T(128)S(1)} %pad_add_fusion.place, f32[32,768]{1,0:T(8,128)S(1)} %shard_map.188.refs_0_, f32[32,768]{1,0:T(8,128)S(1)} %collective-permute-done.8.refs_1_, f32[32,768]{1,0:T(8,128)S(1)} %collective-permute-done.9.refs_2_, ...), custom_call_target="tpu_custom_call" | custom-call | tf_op jit(solution)/shard_map/pallas_call | solution.py:234
  44.2 0.1 collective-permute-start.11
  44.3 0.4 collective-permute-start.16
  44.7 1.5 %collective-permute-start.20 = (f32[64,768]{1,0:T(8,128)S(1)}, f32[64,768]{1,0:T(8,128)S(1)}, u32[]{:S(2)}, u32[]{:S(2)}) collective-permute-start(f32[64,768]{1,0:T(8,128)S(1)} %slice.34), channel_id=1, source_target_pairs={{0,2},{2,0},{4,6},{6,4},{1,3},{3,1},{5,7},{7,5},{8,10},{10,8},{12,... | collective-permute-start | bytes 589832 | tf_op jit(solution)/shard_map/ppermute | solution.py:21
  46.2 0.0 collective-permute-done.17.refs_9_
  46.2 0.3 collective-permute-start.21
  46.5 0.0 collective-permute-done.18.refs_10_
  46.5 1.7 %collective-permute-start.22 = (f32[64,768]{1,0:T(8,128)S(1)}, f32[64,768]{1,0:T(8,128)S(1)}, u32[]{:S(2)}, u32[]{:S(2)}) collective-permute-start(f32[64,768]{1,0:T(8,128)S(1)} %slice.34), channel_id=1, source_target_pairs={{0,6},{2,4},{4,2},{6,0},{1,7},{3,5},{5,3},{7,1},{8,14},{10,12},{12... | collective-permute-start | bytes 589832 | tf_op jit(solution)/shard_map/ppermute | solution.py:21
  48.2 0.0 collective-permute-done.11
  48.2 3.1 %collective-permute-start.19 = (f32[64,768]{1,0:T(8,128)S(1)}, f32[64,768]{1,0:T(8,128)S(1)}, u32[]{:S(2)}, u32[]{:S(2)}) collective-permute-start(f32[64,768]{1,0:T(8,128)S(1)} %pad_maximum_fusion.2.refs_3_), channel_id=1, source_target_pairs={{0,16},{8,24},{16,0},{24,8},{1,17},{9,25},{17,1},{25,9},{2,18},{10... | collective-permute-start | bytes 589832 | tf_op jit(solution)/shard_map/ppermute | solution.py:21
  51.3 1.2 %shard_map.192 = (f32[8,256]{1,0:T(8,128)}, f32[8,256]{1,0:T(8,128)}, f32[8,512]{1,0:T(8,128)}, f32[8,512]{1,0:T(8,128)}) custom-call(s32[2]{0:T(128)S(1)} %pad_add_fusion.place, f32[32,768]{1,0:T(8,128)S(1)} %add.18.mine, f32[32,768]{1,0:T(8,128)S(1)} %collective-permute-done.4.other, f32[80,768]{1,0:T(8,128)S(1)} %get-tuple-element.46.refs_0_.own), custom_call_target="tpu_custom_call" | custom-call | tf_op jit(solution)/shard_map/pallas_call | solution.py:234
  52.4 1.0 %shard_map.190 = (f32[1024,256]{1,0:T(8,128)S(1)}, f32[1024,512]{1,0:T(8,128)S(1)}) custom-call(f32[128,768]{1,0:T(8,128)S(1)} %get-tuple-element.48.whole, bf16[1024,128]{1,0:T(8,128)(2,1)S(1)} %get-tuple-element.38.query_basis, bf16[1024,128]{1,0:T(8,128)(2,1)S(1)} %get-tuple-element.39.value_basis), custom_call_target="tpu_custom_call" | custom-call | tf_op jit(solution)/shard_map/pallas_call | solution.py:234
  53.4 0.0 collective-permute-done.16.refs_7_
  53.4 2.6 %shard_map.191 = (f32[64,256]{1,0:T(8,128)}, f32[64,512]{1,0:T(8,128)}, f32[64,256]{1,0:T(8,128)}, f32[64,512]{1,0:T(8,128)}, bf16[1024,256]{1,0:T(8,128)(2,1)}, /*index=5*/bf16[1024,512]{1,0:T(8,128)(2,1)}) custom-call(s32[2]{0:T(128)S(1)} %pad_add_fusion.place, f32[2,128]{1,0:T(2,128)S(1)} %add.19.sums, f32[1024,256]{1,0:T(8,128)S(1)} %get-tuple-element.49.query_product, ...), custom_call_target="tpu_custom_call" | custom-call | tf_op jit(solution)/shard_map/pallas_call | solution.py:234
  56.0 0.0 collective-permute-done.20.refs_1_
  56.0 1.1 %collective-permute-done.21.refs_2_ = f32[64,768]{1,0:T(8,128)S(1)} collective-permute-done((f32[64,768]{1,0:T(8,128)S(1)}, f32[64,768]{1,0:T(8,128)S(1)}, u32[]{:S(2)}, u32[]{:S(2)}) %collective-permute-start.21) | collective-permute-done | bytes 196640 | tf_op jit(solution)/shard_map/ppermute | solution.py:21
  57.1 0.0 collective-permute-done.22.refs_3_
  57.1 2.8 %collective-permute-done.19.refs_0_ = f32[64,768]{1,0:T(8,128)S(1)} collective-permute-done((f32[64,768]{1,0:T(8,128)S(1)}, f32[64,768]{1,0:T(8,128)S(1)}, u32[]{:S(2)}, u32[]{:S(2)}) %collective-permute-start.19) | collective-permute-done | bytes 196640 | tf_op jit(solution)/shard_map/ppermute | solution.py:21
  60.0 1.4 %shard_map.193 = (bf16[1024,256]{1,0:T(8,128)(2,1)}, bf16[1024,512]{1,0:T(8,128)(2,1)}) custom-call(s32[2]{0:T(128)S(1)} %pad_add_fusion.place, f32[2,128]{1,0:T(2,128)S(1)} %add.19.sums, f32[1024,256]{1,0:T(8,128)S(1)} %get-tuple-element.49.query_product, ...), custom_call_target="tpu_custom_call", output_to_operand_aliasing={{0}: (8, {}), {1}: (9, {})} | custom-call | tf_op jit(solution)/shard_map/pallas_call | solution.py:234
  (11 shorter events, 0.1 us)
Async XLA Ops:
  2.2 13.7 %collective-permute-start.5 = (f32[80,768]{1,0:T(8,128)S(1)}, f32[80,768]{1,0:T(8,128)S(1)}, u32[]{:S(2)}, u32[]{:S(2)}) collective-permute-start(f32[80,768]{1,0:T(8,128)S(1)} %get-tuple-element.46.refs_0_.own), channel_id=1, source_target_pairs={{0,8},{8,0},{16,24},{24,16},{1,9},{9,1},{17,25},{25,17},{2,10},{10... | collective-permute-start | bytes 737288 | tf_op jit(solution)/shard_map/ppermute | solution.py:21
  5.3 7.6 %collective-permute-start.12 = (f32[64,768]{1,0:T(8,128)S(1)}, f32[64,768]{1,0:T(8,128)S(1)}, u32[]{:S(2)}, u32[]{:S(2)}) collective-permute-start(f32[64,768]{1,0:T(8,128)S(1)} %get-tuple-element.51), channel_id=1, source_target_pairs={{0,2},{2,0},{4,6},{6,4},{1,3},{3,1},{5,7},{7,5},{8,10},{10,8},{12,... | collective-permute-start | bytes 589832 | tf_op jit(solution)/shard_map/ppermute | solution.py:21
  6.8 6.6 %collective-permute-start.13 = (f32[64,768]{1,0:T(8,128)S(1)}, f32[64,768]{1,0:T(8,128)S(1)}, u32[]{:S(2)}, u32[]{:S(2)}) collective-permute-start(f32[64,768]{1,0:T(8,128)S(1)} %get-tuple-element.51), channel_id=1, source_target_pairs={{0,4},{2,6},{4,0},{6,2},{1,5},{3,7},{5,1},{7,3},{8,12},{10,14},{12... | collective-permute-start | bytes 589832 | tf_op jit(solution)/shard_map/ppermute | solution.py:21
  8.3 13.1 %collective-permute-start.6 = (f32[80,768]{1,0:T(8,128)S(1)}, f32[80,768]{1,0:T(8,128)S(1)}, u32[]{:S(2)}, u32[]{:S(2)}) collective-permute-start(f32[80,768]{1,0:T(8,128)S(1)} %get-tuple-element.46.refs_0_.own), channel_id=1, source_target_pairs={{0,16},{8,24},{16,0},{24,8},{1,17},{9,25},{17,1},{25,9},{2,18},{10... | collective-permute-start | bytes 737288 | tf_op jit(solution)/shard_map/ppermute | solution.py:21
  12.3 5.0 %collective-permute-start = (f32[32,768]{1,0:T(8,128)S(1)}, f32[32,768]{1,0:T(8,128)S(1)}, u32[]{:S(2)}, u32[]{:S(2)}) collective-permute-start(f32[32,768]{1,0:T(8,128)S(1)} %get-tuple-element.43), channel_id=1, source_target_pairs={{0,2},{2,0},{4,6},{6,4},{1,3},{3,1},{5,7},{7,5},{8,10},{10,8},{12,... | collective-permute-start | bytes 294920 | tf_op jit(solution)/shard_map/ppermute | solution.py:21
  12.9 8.5 %collective-permute-start.1 = (f32[32,768]{1,0:T(8,128)S(1)}, f32[32,768]{1,0:T(8,128)S(1)}, u32[]{:S(2)}, u32[]{:S(2)}) collective-permute-start(f32[32,768]{1,0:T(8,128)S(1)} %get-tuple-element.44), channel_id=1, source_target_pairs={{0,4},{2,6},{4,0},{6,2},{1,5},{3,7},{5,1},{7,3},{8,12},{10,14},{12... | collective-permute-start | bytes 294920 | tf_op jit(solution)/shard_map/ppermute | solution.py:21
  13.4 8.0 %collective-permute-start.2 = (f32[32,768]{1,0:T(8,128)S(1)}, f32[32,768]{1,0:T(8,128)S(1)}, u32[]{:S(2)}, u32[]{:S(2)}) collective-permute-start(f32[32,768]{1,0:T(8,128)S(1)} %get-tuple-element.45), channel_id=1, source_target_pairs={{0,6},{2,4},{4,2},{6,0},{1,7},{3,5},{5,3},{7,1},{8,14},{10,12},{12... | collective-permute-start | bytes 294920 | tf_op jit(solution)/shard_map/ppermute | solution.py:21
  16.0 24.4 %collective-permute-start.14 = (f32[96,768]{1,0:T(8,128)S(1)}, f32[96,768]{1,0:T(8,128)S(1)}, u32[]{:S(2)}, u32[]{:S(2)}) collective-permute-start(f32[96,768]{1,0:T(8,128)S(1)} %get-tuple-element.64), channel_id=1, source_target_pairs={{0,4},{2,6},{4,0},{6,2},{1,5},{3,7},{5,1},{7,3},{8,12},{10,14},{12... | collective-permute-start | bytes 884744 | tf_op jit(solution)/shard_map/ppermute | solution.py:21
  17.3 23.2 %collective-permute-start.15 = (f32[96,768]{1,0:T(8,128)S(1)}, f32[96,768]{1,0:T(8,128)S(1)}, u32[]{:S(2)}, u32[]{:S(2)}) collective-permute-start(f32[96,768]{1,0:T(8,128)S(1)} %get-tuple-element.65), channel_id=1, source_target_pairs={{0,2},{2,0},{4,6},{6,4},{1,3},{3,1},{5,7},{7,5},{8,10},{10,8},{12,... | collective-permute-start | bytes 884744 | tf_op jit(solution)/shard_map/ppermute | solution.py:21
  21.4 14.8 %collective-permute-start.7 = (f32[80,768]{1,0:T(8,128)S(1)}, f32[80,768]{1,0:T(8,128)S(1)}, u32[]{:S(2)}, u32[]{:S(2)}) collective-permute-start(f32[80,768]{1,0:T(8,128)S(1)} %collective-permute-done.6.refs_2_.refs_8_), channel_id=1, source_target_pairs={{0,8},{8,0},{16,24},{24,16},{1,9},{9,1},{17,25},{25,17},{2,10},{10... | collective-permute-start | bytes 737288 | tf_op jit(solution)/shard_map/ppermute | solution.py:21
  21.4 8.3 %collective-permute-start.3 = (f32[32,768]{1,0:T(8,128)S(1)}, f32[32,768]{1,0:T(8,128)S(1)}, u32[]{:S(2)}, u32[]{:S(2)}) collective-permute-start(f32[32,768]{1,0:T(8,128)S(1)} %add_add_fusion), channel_id=1, source_target_pairs={{0,8},{8,0},{16,24},{24,16},{1,9},{9,1},{17,25},{25,17},{2,10},{10... | collective-permute-start | bytes 294920 | tf_op jit(solution)/shard_map/ppermute | solution.py:21
  29.8 6.4 %collective-permute-start.4 = (f32[32,768]{1,0:T(8,128)S(1)}, f32[32,768]{1,0:T(8,128)S(1)}, u32[]{:S(2)}, u32[]{:S(2)}) collective-permute-start(f32[32,768]{1,0:T(8,128)S(1)} %add.18.mine), channel_id=1, source_target_pairs={{0,16},{8,24},{16,0},{24,8},{1,17},{9,25},{17,1},{25,9},{2,18},{10... | collective-permute-start | bytes 294920 | tf_op jit(solution)/shard_map/ppermute | solution.py:21
  36.9 5.6 %collective-permute-start.10 = (f32[32,768]{1,0:T(8,128)S(1)}, f32[32,768]{1,0:T(8,128)S(1)}, u32[]{:S(2)}, u32[]{:S(2)}) collective-permute-start(f32[32,768]{1,0:T(8,128)S(1)} %shard_map.188.refs_0_), channel_id=1, source_target_pairs={{0,6},{2,4},{4,2},{6,0},{1,7},{3,5},{5,3},{7,1},{8,14},{10,12},{12... | collective-permute-start | bytes 294920 | tf_op jit(solution)/shard_map/ppermute | solution.py:21
  36.9 6.1 %collective-permute-start.8 = (f32[32,768]{1,0:T(8,128)S(1)}, f32[32,768]{1,0:T(8,128)S(1)}, u32[]{:S(2)}, u32[]{:S(2)}) collective-permute-start(f32[32,768]{1,0:T(8,128)S(1)} %shard_map.188.refs_0_), channel_id=1, source_target_pairs={{0,2},{2,0},{4,6},{6,4},{1,3},{3,1},{5,7},{7,5},{8,10},{10,8},{12,... | collective-permute-start | bytes 294920 | tf_op jit(solution)/shard_map/ppermute | solution.py:21
  38.1 5.4 %collective-permute-start.9 = (f32[32,768]{1,0:T(8,128)S(1)}, f32[32,768]{1,0:T(8,128)S(1)}, u32[]{:S(2)}, u32[]{:S(2)}) collective-permute-start(f32[32,768]{1,0:T(8,128)S(1)} %shard_map.188.refs_0_), channel_id=1, source_target_pairs={{0,4},{2,6},{4,0},{6,2},{1,5},{3,7},{5,1},{7,3},{8,12},{10,14},{12... | collective-permute-start | bytes 294920 | tf_op jit(solution)/shard_map/ppermute | solution.py:21
  40.4 5.7 %collective-permute-start.17 = (f32[64,768]{1,0:T(8,128)S(1)}, f32[64,768]{1,0:T(8,128)S(1)}, u32[]{:S(2)}, u32[]{:S(2)}) collective-permute-start(f32[64,768]{1,0:T(8,128)S(1)} %slice.33), channel_id=1, source_target_pairs={{0,2},{2,0},{4,6},{6,4},{1,3},{3,1},{5,7},{7,5},{8,10},{10,8},{12,... | collective-permute-start | bytes 589832 | tf_op jit(solution)/shard_map/ppermute | solution.py:21
  40.5 5.9 %collective-permute-start.18 = (f32[64,768]{1,0:T(8,128)S(1)}, f32[64,768]{1,0:T(8,128)S(1)}, u32[]{:S(2)}, u32[]{:S(2)}) collective-permute-start(f32[64,768]{1,0:T(8,128)S(1)} %slice.33), channel_id=1, source_target_pairs={{0,4},{2,6},{4,0},{6,2},{1,5},{3,7},{5,1},{7,3},{8,12},{10,14},{12... | collective-permute-start | bytes 589832 | tf_op jit(solution)/shard_map/ppermute | solution.py:21
  44.2 4.0 %collective-permute-start.11 = (f32[2,128]{1,0:T(2,128)S(1)}, f32[2,128]{1,0:T(2,128)S(1)}, u32[]{:S(2)}, u32[]{:S(2)}) collective-permute-start(f32[2,128]{1,0:T(2,128)S(1)} %get-tuple-element.47), channel_id=1, source_target_pairs={{0,1},{1,0},{2,3},{3,2},{4,5},{5,4},{6,7},{7,6},{8,9},{9,8},{10,11... | collective-permute-start | bytes 3080 | tf_op jit(solution)/shard_map/ppermute | solution.py:21
  44.3 9.1 %collective-permute-start.16 = (f32[64,768]{1,0:T(8,128)S(1)}, f32[64,768]{1,0:T(8,128)S(1)}, u32[]{:S(2)}, u32[]{:S(2)}) collective-permute-start(f32[64,768]{1,0:T(8,128)S(1)} %pad_maximum_fusion.2.refs_3_), channel_id=1, source_target_pairs={{0,8},{8,0},{16,24},{24,16},{1,9},{9,1},{17,25},{25,17},{2,10},{10... | collective-permute-start | bytes 589832 | tf_op jit(solution)/shard_map/ppermute | solution.py:21
  44.7 11.3 %collective-permute-start.20 = (f32[64,768]{1,0:T(8,128)S(1)}, f32[64,768]{1,0:T(8,128)S(1)}, u32[]{:S(2)}, u32[]{:S(2)}) collective-permute-start(f32[64,768]{1,0:T(8,128)S(1)} %slice.34), channel_id=1, source_target_pairs={{0,2},{2,0},{4,6},{6,4},{1,3},{3,1},{5,7},{7,5},{8,10},{10,8},{12,... | collective-permute-start | bytes 589832 | tf_op jit(solution)/shard_map/ppermute | solution.py:21
  46.2 11.0 %collective-permute-start.21 = (f32[64,768]{1,0:T(8,128)S(1)}, f32[64,768]{1,0:T(8,128)S(1)}, u32[]{:S(2)}, u32[]{:S(2)}) collective-permute-start(f32[64,768]{1,0:T(8,128)S(1)} %slice.34), channel_id=1, source_target_pairs={{0,4},{2,6},{4,0},{6,2},{1,5},{3,7},{5,1},{7,3},{8,12},{10,14},{12... | collective-permute-start | bytes 589832 | tf_op jit(solution)/shard_map/ppermute | solution.py:21
  46.5 10.7 %collective-permute-start.22 = (f32[64,768]{1,0:T(8,128)S(1)}, f32[64,768]{1,0:T(8,128)S(1)}, u32[]{:S(2)}, u32[]{:S(2)}) collective-permute-start(f32[64,768]{1,0:T(8,128)S(1)} %slice.34), channel_id=1, source_target_pairs={{0,6},{2,4},{4,2},{6,0},{1,7},{3,5},{5,3},{7,1},{8,14},{10,12},{12... | collective-permute-start | bytes 589832 | tf_op jit(solution)/shard_map/ppermute | solution.py:21
  48.2 11.8 %collective-permute-start.19 = (f32[64,768]{1,0:T(8,128)S(1)}, f32[64,768]{1,0:T(8,128)S(1)}, u32[]{:S(2)}, u32[]{:S(2)}) collective-permute-start(f32[64,768]{1,0:T(8,128)S(1)} %pad_maximum_fusion.2.refs_3_), channel_id=1, source_target_pairs={{0,16},{8,24},{16,0},{24,8},{1,17},{9,25},{17,1},{25,9},{2,18},{10... | collective-permute-start | bytes 589832 | tf_op jit(solution)/shard_map/ppermute | solution.py:21

commit v2 on v1

--- a/solution.py
+++ b/solution.py
@@ -109,21 +109,6 @@
         )[2]
 
 
-def record_kernel(counts, place, mine, other, own, *refs):
-    rows, ranks, query_width = counts
-    query_first, query_second, value_first, value_second = refs
-    where = aligned(place[0], ranks)
-    first, second, _ = moments(
-        mine[where, :] + other[where, :],
-        own[rows : rows + ranks, :],
-        own[rows + ranks : rows + 2 * ranks, :],
-    )
-    query_first[...] = first[:, :query_width]
-    query_second[...] = second[:, :query_width]
-    value_first[...] = first[:, query_width:]
-    value_second[...] = second[:, query_width:]
-
-
 def whole_kernel(counts, place, *refs):
     fs, rep, ranks, query_width = counts
     blocks, (whole, sums) = refs[:rep], refs[rep:]
@@ -157,45 +142,78 @@
         )
 
 
-def finish_kernel(counts, pieces, place, sums, query_product, value_product, *refs):
+def scales(sums, entries):
+    return [1.0 / jnp.sqrt(sums[i : i + 1, 0:1] / entries[i] + 1.0) for i in range(2)]
+
+
+def early_kernel(counts, pieces, place, sums, query_product, value_product, *refs):
     rep, rows, entries, blocks = counts
-    sources, refs = refs[:blocks], refs[blocks:]
+    sources, held = refs[:blocks], refs[blocks:]
     z, r = place[0], place[1]
-    query_width = query_product.shape[1]
-    query_scale = 1.0 / jnp.sqrt(sums[0:1, 0:1] / entries[0] + 1.0)
-    value_scale = 1.0 / jnp.sqrt(sums[1:2, 0:1] / entries[1] + 1.0)
-    own = any(kz == 0 and kr == 0 for kz, kr, *_ in pieces)
-    if own:
-        query_update, value_update, query_new, value_new, query_copy, value_copy = refs[:6]
-        updates, news = (query_update, value_update), (query_new, value_new)
-        refs = refs[6:]
-    else:
-        query_copy, value_copy = refs[2:4]
-        refs = refs[4:]
-    query_held, value_held, sems = refs
-    copies = []
+    factors = scales(sums, entries)
     filled = 0
     for kz, kr, source, start, offset, size in pieces:
         owner = (z ^ kz) * rep + (r ^ kr)
         where = pl.ds(pl.multiple_of(owner * rows + offset, size), size)
-        slot = pl.ds(filled, size)
-        for i, (product, scale, lo, held, copy) in enumerate(
-            (
-                (query_product, query_scale, 0, query_held, query_copy),
-                (value_product, value_scale, query_width, value_held, value_copy),
+        lo = 0
+        for product, factor, out in zip((query_product, value_product), factors, held):
+            old = sources[source][start : start + size, lo : lo + product.shape[1]]
+            weight = old - 0.01 * (product[where, :] * factor)
+            out[filled : filled + size, :] = weight.astype(BF16)
+            lo += product.shape[1]
+        filled += size
+
+
+def late_kernel(counts, ready, pieces, place, sums, query_product, value_product, *refs):
+    rep, rows, entries, blocks, ranks = counts
+    early, sources, (mine, other) = refs[:2], refs[2 : 2 + blocks], refs[2 + blocks : 4 + blocks]
+    outs, refs = refs[4 + blocks : 14 + blocks], refs[14 + blocks :]
+    copy_outs, (held, staged, sems) = outs[8:], (refs[:2], refs[2:10], refs[10])
+    z, r = place[0], place[1]
+    query_width = query_product.shape[1]
+    copies = []
+
+    def send(source, target):
+        copies.append(pltpu.make_async_copy(source, target, sems.at[len(copies)]))
+        copies[-1].start()
+
+    def target_rows(kz, kr, offset, size):
+        owner = (z ^ kz) * rep + (r ^ kr)
+        return pl.ds(pl.multiple_of(owner * rows + offset, size), size)
+
+    filled = 0
+    for kz, kr, _, _, offset, size in ready:
+        for source, out in zip(early, copy_outs):
+            send(source.at[pl.ds(filled, size), :], out.at[target_rows(kz, kr, offset, size), :])
+        filled += size
+    factors = scales(sums, entries)
+    filled = 0
+    for kz, kr, source, start, offset, size in pieces:
+        where = target_rows(kz, kr, offset, size)
+        lo = 0
+        for i, product in enumerate((query_product, value_product)):
+            step = product[where, :] * factors[i]
+            weight = sources[source][start : start + size, lo : lo + product.shape[1]] - 0.01 * step
+            held[i][filled : filled + size, :] = weight.astype(BF16)
+            send(held[i].at[pl.ds(filled, size), :], copy_outs[i].at[where, :])
+            lo += product.shape[1]
+            if kz == 0 and kr == 0:
+                staged[i][...] = step
+                staged[2 + i][...] = weight
+                send(staged[i], outs[i])
+                send(staged[2 + i], outs[2 + i])
+        if kz == 0 and kr == 0:
+            where = aligned(z, ranks)
+            first, second, _ = moments(
+                mine[where, :] + other[where, :],
+                sources[source][rows : rows + ranks, :],
+                sources[source][rows + ranks : rows + 2 * ranks, :],
             )
-        ):
-            step = product[where, :] * scale
-            old = sources[source][start : start + size, lo : lo + product.shape[1]]
-            weight = old - 0.01 * step
-            held[slot, :] = weight.astype(BF16)
-            if kz == 0 and kr == 0:
-                updates[i][...] = step
-                news[i][...] = weight
-            copies.append(
-                pltpu.make_async_copy(held.at[slot, :], copy.at[where, :], sems.at[len(copies)])
-            )
-            copies[-1].start()
+            parts = (first[:, :query_width], second[:, :query_width])
+            parts += (first[:, query_width:], second[:, query_width:])
+            for i, part in enumerate(parts):
+                staged[4 + i][...] = part
+                send(staged[4 + i], outs[4 + i])
         filled += size
     for copy in copies:
         copy.wait()
@@ -307,14 +325,6 @@
         *along,
     )
     wholes = spread(direction, "rep")
-    new_moments = call(
-        functools.partial(record_kernel, (rows, ranks, query_width)),
-        (shape(ranks, query_width),) * 2 + (shape(ranks, value_width),) * 2,
-        place,
-        mine,
-        other,
-        own,
-    )
     whole, sums = call(
         functools.partial(whole_kernel, (fs, rep, ranks, query_width)),
         (shape(fs * rep * ranks, width), shape(2, 128)),
@@ -334,66 +344,57 @@
     )
 
     entries = (fs * rep * ranks * query_width * tp, fs * rep * ranks * value_width * tp)
-    copy_shapes = (shape(total, query_width, dtype=BF16), shape(total, value_width, dtype=BF16))
-
-    def finish(pieces, copies=None):
+
+    def indexed(pieces):
         sources = []
         for piece in pieces:
             if not any(piece[2] is source for source in sources):
                 sources.append(piece[2])
         found = [[i for i, s in enumerate(sources) if s is piece[2]][0] for piece in pieces]
-        pieces = [(p[0], p[1], i, *p[3:]) for p, i in zip(pieces, found)]
-        held = sum(piece[-1] for piece in pieces)
-        first = 4 + len(sources)
-        kernel = functools.partial(finish_kernel, (rep, rows, entries, len(sources)), pieces)
-        scratch = [
-            pltpu.VMEM((held, query_width), BF16),
-            pltpu.VMEM((held, value_width), BF16),
-            pltpu.SemaphoreType.DMA((2 * len(pieces),)),
-        ]
-        if copies is None:
-            shapes = (shape(rows, query_width), shape(rows, value_width)) * 2 + copy_shapes
-            return call(
-                kernel, shapes, place, sums, *products, *sources, scratch=scratch, outside_out=(4, 5)
-            )
-        return call(
-            kernel,
-            copy_shapes,
-            place,
-            sums,
-            *products,
-            *sources,
-            *copies,
-            scratch=scratch,
-            outside=(first, first + 1),
-            outside_out=(0, 1),
-            aliases={first: 0, first + 1: 1},
-        )
-
-    early, late = [], []
+        return sources, [(p[0], p[1], i, *p[3:]) for p, i in zip(pieces, found)]
+
+    early, late = [], [(0, 0, own, 0, 0, rows)]
     for kz in range(fs):
         group = late if kz == fs - 1 else early
-        early.append((kz, 0, along[kz], 0, 0, rows))
+        if kz > 0:
+            early.append((kz, 0, along[kz], 0, 0, rows))
         for kr in (1, 2):
             group.append((kz, kr, far[kz][kr - 1], 0, 0, rows))
         if kz == fs - 1:
             late.append((kz, 3, far[kz][2], 0, 0, rows))
         else:
             (late if kz == fs - 2 else early).append((kz, 3, ([cross] + crosses)[kz], 0, 0, rows))
-    query_update, value_update, query_new, value_new, *copies = finish(early)
-    query_copy, value_copy = finish(late, copies)
-    query_first_new, query_second_new, value_first_new, value_second_new = new_moments
-    return (
-        query_update,
-        value_update,
-        query_new,
-        value_new,
-        query_first_new,
-        query_second_new,
-        value_first_new,
-        value_second_new,
-        query_copy,
-        value_copy,
+
+    def halves(count, dtype=F32):
+        return (shape(count, query_width, dtype=dtype), shape(count, value_width, dtype=dtype))
+
+    sources, early = indexed(early)
+    early_rows = sum(piece[-1] for piece in early)
+    ready = call(
+        functools.partial(early_kernel, (rep, rows, entries, len(sources)), early),
+        halves(early_rows, BF16),
+        place,
+        sums,
+        *products,
+        *sources,
+    )
+    sources, late = indexed(late)
+    moment_shapes = (shape(ranks, query_width),) * 2 + (shape(ranks, value_width),) * 2
+    shapes = halves(rows) * 2 + moment_shapes
+    late_rows = sum(piece[-1] for piece in late)
+    return call(
+        functools.partial(late_kernel, (rep, rows, entries, len(sources), ranks), early, late),
+        shapes + halves(total, BF16),
+        place,
+        sums,
+        *products,
+        *ready,
+        *sources,
+        mine,
+        other,
+        scratch=[pltpu.VMEM(s.shape, s.dtype) for s in halves(late_rows, BF16) + shapes]
+        + [pltpu.SemaphoreType.DMA((2 * len(early) + 2 * len(late) + 8,))],
+        outside_out=range(10),
     )
 
 

time: 61.5 us -> 62.3 us (1.013)
  waiting for transfers between devices: 20 us -> 22.9 us
  Pallas kernels: 10.3 us -> 8.16 us
    ppermute x23, waiting for transfers between devices: 20 us -> 22.9 us  [swap(): return lax.ppermute(block, axis, pairs)]
    pallas_call x8 -> x7, Pallas kernels: 10.3 us -> 8.16 us  [call(): pl.pallas_call(kernel, out_shape=out_shape, in_specs=specs, out_specs=tup...]
  transfers between devices with their start and end apart: 23 -> 23, of which waited for: 9 -> 10; matrix products, arithmetic and copies ran while one was open for 0% -> 0% of each run, Pallas kernels for 12% -> 7%
where the time goes in v2:
time: 62.3 us; the launch traced here: 62.1 us
  starting transfers between devices  30 us (48%)
  waiting for transfers between devices  22.9 us (37%)
  Pallas kernels  8.16 us (13%)
  between operations  0.83 us (1%)
    ppermute x23, starting transfers between devices, swap(): return lax.ppermute(block, axis, pairs)  30 us
    ppermute x23, waiting for transfers between devices, swap(): return lax.ppermute(block, axis, pairs)  22.9 us
    pallas_call x7, Pallas kernels, call(): pl.pallas_call(kernel, out_shape=out_shape, in_specs=specs, out_specs=tup...  8.16 us
  transfers between devices with their start and end apart: 23, of which 10 were waited for; matrix products, arithmetic and copies ran while one was open for 0% of the time, Pallas kernels for 7%

profile of v2, /device:TPU:0, one launch (start us, length us, event | category | flops | bytes accessed | tf_op | source)
XLA Modules:
  0.0 62.1 jit_solution(5272009427867172293)
XLA Ops:
  0.6 1.5 %shard_map.186 = (f32[64,768]{1,0:T(8,128)S(1)}, f32[80,768]{1,0:T(8,128)S(1)}, bf16[128,1024]{1,0:T(8,128)(2,1)S(1)}, bf16[1024,128]{1,0:T(8,128)(2,1)S(1)}, bf...) custom-call(f32[64,256]{1,0:T(8,128)} %refs_0_.1, f32[64,512]{1,0:T(8,128)} %refs_1_.1, ...), custom_call_target="tpu_custom_call" | custom-call | tf_op jit(solution)/shard_map/pallas_call | solution.py:252
  2.2 3.1 %collective-permute-start.5 = (f32[80,768]{1,0:T(8,128)S(1)}, f32[80,768]{1,0:T(8,128)S(1)}, u32[]{:S(2)}, u32[]{:S(2)}) collective-permute-start(f32[80,768]{1,0:T(8,128)S(1)} %get-tuple-element.36.refs_0_.refs_2_), channel_id=1, source_target_pairs={{0,8},{8,0},{16,24},{24,16},{1,9},{9,1},{17,25},{25,17},{2,10},{10... | collective-permute-start | bytes 737288 | tf_op jit(solution)/shard_map/ppermute | solution.py:21
  5.3 1.5 %collective-permute-start.12 = (f32[64,768]{1,0:T(8,128)S(1)}, f32[64,768]{1,0:T(8,128)S(1)}, u32[]{:S(2)}, u32[]{:S(2)}) collective-permute-start(f32[64,768]{1,0:T(8,128)S(1)} %get-tuple-element.41), channel_id=1, source_target_pairs={{0,2},{2,0},{4,6},{6,4},{1,3},{3,1},{5,7},{7,5},{8,10},{10,8},{12,... | collective-permute-start | bytes 589832 | tf_op jit(solution)/shard_map/ppermute | solution.py:21
  6.8 1.5 %collective-permute-start.13 = (f32[64,768]{1,0:T(8,128)S(1)}, f32[64,768]{1,0:T(8,128)S(1)}, u32[]{:S(2)}, u32[]{:S(2)}) collective-permute-start(f32[64,768]{1,0:T(8,128)S(1)} %get-tuple-element.41), channel_id=1, source_target_pairs={{0,4},{2,6},{4,0},{6,2},{1,5},{3,7},{5,1},{7,3},{8,12},{10,14},{12... | collective-permute-start | bytes 589832 | tf_op jit(solution)/shard_map/ppermute | solution.py:21
  8.3 2.6 %collective-permute-start.6 = (f32[80,768]{1,0:T(8,128)S(1)}, f32[80,768]{1,0:T(8,128)S(1)}, u32[]{:S(2)}, u32[]{:S(2)}) collective-permute-start(f32[80,768]{1,0:T(8,128)S(1)} %get-tuple-element.36.refs_0_.refs_2_), channel_id=1, source_target_pairs={{0,16},{8,24},{16,0},{24,8},{1,17},{9,25},{17,1},{25,9},{2,18},{10... | collective-permute-start | bytes 737288 | tf_op jit(solution)/shard_map/ppermute | solution.py:21
  10.9 0.1 pad_add_fusion.place
  11.0 1.3 %shard_map.187 = (f32[32,768]{1,0:T(8,128)S(1)}, f32[32,768]{1,0:T(8,128)S(1)}, f32[32,768]{1,0:T(8,128)S(1)}, f32[32,768]{1,0:T(8,128)S(1)}) custom-call(s32[2]{0:T(128)S(1)} %pad_add_fusion.place, bf16[128,1024]{1,0:T(8,128)(2,1)S(1)} %get-tuple-element.27.tokens, bf16[1024,128]{1,0:T(8,128)(2,1)S(1)} %get-tuple-element.28.query_basis, ...), custom_call_target="tpu_custom_call" | custom-call | tf_op jit(solution)/shard_map/pallas_call | solution.py:252
  12.3 0.6 collective-permute-start
  12.9 0.0 collective-permute-done.12.refs_0_
  12.9 0.5 collective-permute-start.1
  13.4 0.0 collective-permute-done.13.refs_1_
  13.4 2.5 %collective-permute-start.2 = (f32[32,768]{1,0:T(8,128)S(1)}, f32[32,768]{1,0:T(8,128)S(1)}, u32[]{:S(2)}, u32[]{:S(2)}) collective-permute-start(f32[32,768]{1,0:T(8,128)S(1)} %get-tuple-element.35), channel_id=1, source_target_pairs={{0,6},{2,4},{4,2},{6,0},{1,7},{3,5},{5,3},{7,1},{8,14},{10,12},{12... | collective-permute-start | bytes 294920 | tf_op jit(solution)/shard_map/ppermute | solution.py:21
  15.9 0.0 collective-permute-done.5.refs_1_.refs_3_
  16.0 0.8 %collective-permute-start.14 = (f32[96,768]{1,0:T(8,128)S(1)}, f32[96,768]{1,0:T(8,128)S(1)}, u32[]{:S(2)}, u32[]{:S(2)}) collective-permute-start(f32[96,768]{1,0:T(8,128)S(1)} %get-tuple-element.44), channel_id=1, source_target_pairs={{0,4},{2,6},{4,0},{6,2},{1,5},{3,7},{5,1},{7,3},{8,12},{10,14},{12... | collective-permute-start | bytes 884744 | tf_op jit(solution)/shard_map/ppermute | solution.py:21
  16.8 0.5 collective-permute-done
  17.3 2.0 %collective-permute-start.15 = (f32[96,768]{1,0:T(8,128)S(1)}, f32[96,768]{1,0:T(8,128)S(1)}, u32[]{:S(2)}, u32[]{:S(2)}) collective-permute-start(f32[96,768]{1,0:T(8,128)S(1)} %get-tuple-element.45), channel_id=1, source_target_pairs={{0,2},{2,0},{4,6},{6,4},{1,3},{3,1},{5,7},{7,5},{8,10},{10,8},{12,... | collective-permute-start | bytes 884744 | tf_op jit(solution)/shard_map/ppermute | solution.py:21
  19.2 2.1 %collective-permute-done.6.refs_2_.refs_7_ = f32[80,768]{1,0:T(8,128)S(1)} collective-permute-done((f32[80,768]{1,0:T(8,128)S(1)}, f32[80,768]{1,0:T(8,128)S(1)}, u32[]{:S(2)}, u32[]{:S(2)}) %collective-permute-start.6) | collective-permute-done | bytes 245792 | tf_op jit(solution)/shard_map/ppermute | solution.py:21
  21.4 0.0 collective-permute-start.7
  21.4 0.0 collective-permute-done.1
  21.4 0.0 collective-permute-done.2
  21.4 2.1 %collective-permute-start.3 = (f32[32,768]{1,0:T(8,128)S(1)}, f32[32,768]{1,0:T(8,128)S(1)}, u32[]{:S(2)}, u32[]{:S(2)}) collective-permute-start(f32[32,768]{1,0:T(8,128)S(1)} %add_add_fusion), channel_id=1, source_target_pairs={{0,8},{8,0},{16,24},{24,16},{1,9},{9,1},{17,25},{25,17},{2,10},{10... | collective-permute-start | bytes 294920 | tf_op jit(solution)/shard_map/ppermute | solution.py:21
  23.5 6.2 %collective-permute-done.3 = f32[32,768]{1,0:T(8,128)S(1)} collective-permute-done((f32[32,768]{1,0:T(8,128)S(1)}, f32[32,768]{1,0:T(8,128)S(1)}, u32[]{:S(2)}, u32[]{:S(2)}) %collective-permute-start.3) | collective-permute-done | bytes 98336 | tf_op jit(solution)/shard_map/ppermute | solution.py:21
  29.8 1.6 %collective-permute-start.4 = (f32[32,768]{1,0:T(8,128)S(1)}, f32[32,768]{1,0:T(8,128)S(1)}, u32[]{:S(2)}, u32[]{:S(2)}) collective-permute-start(f32[32,768]{1,0:T(8,128)S(1)} %add.18.mine.refs_7_), channel_id=1, source_target_pairs={{0,16},{8,24},{16,0},{24,8},{1,17},{9,25},{17,1},{25,9},{2,18},{10... | collective-permute-start | bytes 294920 | tf_op jit(solution)/shard_map/ppermute | solution.py:21
  31.4 4.8 %collective-permute-done.4.other.refs_8_ = f32[32,768]{1,0:T(8,128)S(1)} collective-permute-done((f32[32,768]{1,0:T(8,128)S(1)}, f32[32,768]{1,0:T(8,128)S(1)}, u32[]{:S(2)}, u32[]{:S(2)}) %collective-permute-start.4) | collective-permute-done | bytes 98336 | tf_op jit(solution)/shard_map/ppermute | solution.py:21
  36.2 0.0 collective-permute-done.7.refs_3_.refs_10_
  36.2 0.6 shard_map.188.refs_0_
  36.9 0.1 collective-permute-start.10
  36.9 1.1 %collective-permute-start.8 = (f32[32,768]{1,0:T(8,128)S(1)}, f32[32,768]{1,0:T(8,128)S(1)}, u32[]{:S(2)}, u32[]{:S(2)}) collective-permute-start(f32[32,768]{1,0:T(8,128)S(1)} %shard_map.188.refs_0_), channel_id=1, source_target_pairs={{0,2},{2,0},{4,6},{6,4},{1,3},{3,1},{5,7},{7,5},{8,10},{10,8},{12,... | collective-permute-start | bytes 294920 | tf_op jit(solution)/shard_map/ppermute | solution.py:21
  38.1 2.3 %collective-permute-start.9 = (f32[32,768]{1,0:T(8,128)S(1)}, f32[32,768]{1,0:T(8,128)S(1)}, u32[]{:S(2)}, u32[]{:S(2)}) collective-permute-start(f32[32,768]{1,0:T(8,128)S(1)} %shard_map.188.refs_0_), channel_id=1, source_target_pairs={{0,4},{2,6},{4,0},{6,2},{1,5},{3,7},{5,1},{7,3},{8,12},{10,14},{12... | collective-permute-start | bytes 294920 | tf_op jit(solution)/shard_map/ppermute | solution.py:21
  40.4 0.0 collective-permute-done.14.refs_5_
  40.4 0.1 collective-permute-start.17
  40.5 0.0 collective-permute-done.15.refs_4_
  40.5 0.6 %collective-permute-start.18 = (f32[64,768]{1,0:T(8,128)S(1)}, f32[64,768]{1,0:T(8,128)S(1)}, u32[]{:S(2)}, u32[]{:S(2)}) collective-permute-start(f32[64,768]{1,0:T(8,128)S(1)} %slice.33), channel_id=1, source_target_pairs={{0,4},{2,6},{4,0},{6,2},{1,5},{3,7},{5,1},{7,3},{8,12},{10,14},{12... | collective-permute-start | bytes 589832 | tf_op jit(solution)/shard_map/ppermute | solution.py:21
  41.2 1.3 %collective-permute-done.10.refs_3_ = f32[32,768]{1,0:T(8,128)S(1)} collective-permute-done((f32[32,768]{1,0:T(8,128)S(1)}, f32[32,768]{1,0:T(8,128)S(1)}, u32[]{:S(2)}, u32[]{:S(2)}) %collective-permute-start.10) | collective-permute-done | bytes 98336 | tf_op jit(solution)/shard_map/ppermute | solution.py:21
  42.5 0.6 collective-permute-done.8.refs_1_
  43.1 0.4 collective-permute-done.9.refs_2_
  43.5 0.7 %shard_map.189 = (f32[128,768]{1,0:T(8,128)S(1)}, f32[2,128]{1,0:T(2,128)S(1)}) custom-call(s32[2]{0:T(128)S(1)} %pad_add_fusion.place, f32[32,768]{1,0:T(8,128)S(1)} %shard_map.188.refs_0_, f32[32,768]{1,0:T(8,128)S(1)} %collective-permute-done.8.refs_1_, f32[32,768]{1,0:T(8,128)S(1)} %collective-permute-done.9.refs_2_, ...), custom_call_target="tpu_custom_call" | custom-call | tf_op jit(solution)/shard_map/pallas_call | solution.py:252
  44.2 0.1 collective-permute-start.11
  44.3 0.4 collective-permute-start.16
  44.7 1.5 %collective-permute-start.20 = (f32[64,768]{1,0:T(8,128)S(1)}, f32[64,768]{1,0:T(8,128)S(1)}, u32[]{:S(2)}, u32[]{:S(2)}) collective-permute-start(f32[64,768]{1,0:T(8,128)S(1)} %slice.34), channel_id=1, source_target_pairs={{0,2},{2,0},{4,6},{6,4},{1,3},{3,1},{5,7},{7,5},{8,10},{10,8},{12,... | collective-permute-start | bytes 589832 | tf_op jit(solution)/shard_map/ppermute | solution.py:21
  46.2 0.0 collective-permute-done.17.refs_8_
  46.2 0.3 collective-permute-start.21
  46.5 0.0 collective-permute-done.18.refs_9_
  46.5 1.7 %collective-permute-start.22 = (f32[64,768]{1,0:T(8,128)S(1)}, f32[64,768]{1,0:T(8,128)S(1)}, u32[]{:S(2)}, u32[]{:S(2)}) collective-permute-start(f32[64,768]{1,0:T(8,128)S(1)} %slice.34), channel_id=1, source_target_pairs={{0,6},{2,4},{4,2},{6,0},{1,7},{3,5},{5,3},{7,1},{8,14},{10,12},{12... | collective-permute-start | bytes 589832 | tf_op jit(solution)/shard_map/ppermute | solution.py:21
  48.2 0.0 collective-permute-done.11
  48.2 3.1 %collective-permute-start.19 = (f32[64,768]{1,0:T(8,128)S(1)}, f32[64,768]{1,0:T(8,128)S(1)}, u32[]{:S(2)}, u32[]{:S(2)}) collective-permute-start(f32[64,768]{1,0:T(8,128)S(1)} %pad_maximum_fusion.2.refs_2_), channel_id=1, source_target_pairs={{0,16},{8,24},{16,0},{24,8},{1,17},{9,25},{17,1},{25,9},{2,18},{10... | collective-permute-start | bytes 589832 | tf_op jit(solution)/shard_map/ppermute | solution.py:21
  51.3 1.0 %shard_map.190 = (f32[1024,256]{1,0:T(8,128)S(1)}, f32[1024,512]{1,0:T(8,128)S(1)}) custom-call(f32[128,768]{1,0:T(8,128)S(1)} %get-tuple-element.38.whole, bf16[1024,128]{1,0:T(8,128)(2,1)S(1)} %get-tuple-element.28.query_basis, bf16[1024,128]{1,0:T(8,128)(2,1)S(1)} %get-tuple-element.29.value_basis), custom_call_target="tpu_custom_call" | custom-call | tf_op jit(solution)/shard_map/pallas_call | solution.py:252
  52.3 0.6 collective-permute-done.16.refs_6_
  52.8 0.9 %shard_map.191 = (bf16[704,256]{1,0:T(8,128)(2,1)S(1)}, bf16[704,512]{1,0:T(8,128)(2,1)S(1)}) custom-call(s32[2]{0:T(128)S(1)} %pad_add_fusion.place, f32[2,128]{1,0:T(2,128)S(1)} %add.19.sums, f32[1024,256]{1,0:T(8,128)S(1)} %get-tuple-element.39.query_product, f32[1024,512]{1,0:T(8,128)S(1)} %get-tuple-element.40.value_product, ...), custom_call_target="tpu_custom_call" | custom-call | tf_op jit(solution)/shard_map/pallas_call | solution.py:252
  53.7 0.0 collective-permute-done.20.refs_4_
  53.7 3.4 %collective-permute-done.21.refs_5_ = f32[64,768]{1,0:T(8,128)S(1)} collective-permute-done((f32[64,768]{1,0:T(8,128)S(1)}, f32[64,768]{1,0:T(8,128)S(1)}, u32[]{:S(2)}, u32[]{:S(2)}) %collective-permute-start.21) | collective-permute-done | bytes 196640 | tf_op jit(solution)/shard_map/ppermute | solution.py:21
  57.1 0.0 collective-permute-done.22.refs_6_
  57.1 2.8 %collective-permute-done.19.refs_3_ = f32[64,768]{1,0:T(8,128)S(1)} collective-permute-done((f32[64,768]{1,0:T(8,128)S(1)}, f32[64,768]{1,0:T(8,128)S(1)}, u32[]{:S(2)}, u32[]{:S(2)}) %collective-permute-start.19) | collective-permute-done | bytes 196640 | tf_op jit(solution)/shard_map/ppermute | solution.py:21
  60.0 2.2 %shard_map.192 = (f32[64,256]{1,0:T(8,128)}, f32[64,512]{1,0:T(8,128)}, f32[64,256]{1,0:T(8,128)}, f32[64,512]{1,0:T(8,128)}, f32[8,256]{1,0:T(8,128)}, /*index=...) custom-call(s32[2]{0:T(128)S(1)} %pad_add_fusion.place, ...), custom_call_target="tpu_custom_call" | custom-call | tf_op jit(solution)/shard_map/pallas_call | solution.py:252
  (12 shorter events, 0.2 us)
Async XLA Ops:
  2.2 13.7 %collective-permute-start.5 = (f32[80,768]{1,0:T(8,128)S(1)}, f32[80,768]{1,0:T(8,128)S(1)}, u32[]{:S(2)}, u32[]{:S(2)}) collective-permute-start(f32[80,768]{1,0:T(8,128)S(1)} %get-tuple-element.36.refs_0_.refs_2_), channel_id=1, source_target_pairs={{0,8},{8,0},{16,24},{24,16},{1,9},{9,1},{17,25},{25,17},{2,10},{10... | collective-permute-start | bytes 737288 | tf_op jit(solution)/shard_map/ppermute | solution.py:21
  5.3 7.6 %collective-permute-start.12 = (f32[64,768]{1,0:T(8,128)S(1)}, f32[64,768]{1,0:T(8,128)S(1)}, u32[]{:S(2)}, u32[]{:S(2)}) collective-permute-start(f32[64,768]{1,0:T(8,128)S(1)} %get-tuple-element.41), channel_id=1, source_target_pairs={{0,2},{2,0},{4,6},{6,4},{1,3},{3,1},{5,7},{7,5},{8,10},{10,8},{12,... | collective-permute-start | bytes 589832 | tf_op jit(solution)/shard_map/ppermute | solution.py:21
  6.8 6.6 %collective-permute-start.13 = (f32[64,768]{1,0:T(8,128)S(1)}, f32[64,768]{1,0:T(8,128)S(1)}, u32[]{:S(2)}, u32[]{:S(2)}) collective-permute-start(f32[64,768]{1,0:T(8,128)S(1)} %get-tuple-element.41), channel_id=1, source_target_pairs={{0,4},{2,6},{4,0},{6,2},{1,5},{3,7},{5,1},{7,3},{8,12},{10,14},{12... | collective-permute-start | bytes 589832 | tf_op jit(solution)/shard_map/ppermute | solution.py:21
  8.3 13.1 %collective-permute-start.6 = (f32[80,768]{1,0:T(8,128)S(1)}, f32[80,768]{1,0:T(8,128)S(1)}, u32[]{:S(2)}, u32[]{:S(2)}) collective-permute-start(f32[80,768]{1,0:T(8,128)S(1)} %get-tuple-element.36.refs_0_.refs_2_), channel_id=1, source_target_pairs={{0,16},{8,24},{16,0},{24,8},{1,17},{9,25},{17,1},{25,9},{2,18},{10... | collective-permute-start | bytes 737288 | tf_op jit(solution)/shard_map/ppermute | solution.py:21
  12.3 5.0 %collective-permute-start = (f32[32,768]{1,0:T(8,128)S(1)}, f32[32,768]{1,0:T(8,128)S(1)}, u32[]{:S(2)}, u32[]{:S(2)}) collective-permute-start(f32[32,768]{1,0:T(8,128)S(1)} %get-tuple-element.33), channel_id=1, source_target_pairs={{0,2},{2,0},{4,6},{6,4},{1,3},{3,1},{5,7},{7,5},{8,10},{10,8},{12,... | collective-permute-start | bytes 294920 | tf_op jit(solution)/shard_map/ppermute | solution.py:21
  12.9 8.5 %collective-permute-start.1 = (f32[32,768]{1,0:T(8,128)S(1)}, f32[32,768]{1,0:T(8,128)S(1)}, u32[]{:S(2)}, u32[]{:S(2)}) collective-permute-start(f32[32,768]{1,0:T(8,128)S(1)} %get-tuple-element.34), channel_id=1, source_target_pairs={{0,4},{2,6},{4,0},{6,2},{1,5},{3,7},{5,1},{7,3},{8,12},{10,14},{12... | collective-permute-start | bytes 294920 | tf_op jit(solution)/shard_map/ppermute | solution.py:21
  13.4 8.0 %collective-permute-start.2 = (f32[32,768]{1,0:T(8,128)S(1)}, f32[32,768]{1,0:T(8,128)S(1)}, u32[]{:S(2)}, u32[]{:S(2)}) collective-permute-start(f32[32,768]{1,0:T(8,128)S(1)} %get-tuple-element.35), channel_id=1, source_target_pairs={{0,6},{2,4},{4,2},{6,0},{1,7},{3,5},{5,3},{7,1},{8,14},{10,12},{12... | collective-permute-start | bytes 294920 | tf_op jit(solution)/shard_map/ppermute | solution.py:21
  16.0 24.4 %collective-permute-start.14 = (f32[96,768]{1,0:T(8,128)S(1)}, f32[96,768]{1,0:T(8,128)S(1)}, u32[]{:S(2)}, u32[]{:S(2)}) collective-permute-start(f32[96,768]{1,0:T(8,128)S(1)} %get-tuple-element.44), channel_id=1, source_target_pairs={{0,4},{2,6},{4,0},{6,2},{1,5},{3,7},{5,1},{7,3},{8,12},{10,14},{12... | collective-permute-start | bytes 884744 | tf_op jit(solution)/shard_map/ppermute | solution.py:21
  17.3 23.2 %collective-permute-start.15 = (f32[96,768]{1,0:T(8,128)S(1)}, f32[96,768]{1,0:T(8,128)S(1)}, u32[]{:S(2)}, u32[]{:S(2)}) collective-permute-start(f32[96,768]{1,0:T(8,128)S(1)} %get-tuple-element.45), channel_id=1, source_target_pairs={{0,2},{2,0},{4,6},{6,4},{1,3},{3,1},{5,7},{7,5},{8,10},{10,8},{12,... | collective-permute-start | bytes 884744 | tf_op jit(solution)/shard_map/ppermute | solution.py:21
  21.4 14.8 %collective-permute-start.7 = (f32[80,768]{1,0:T(8,128)S(1)}, f32[80,768]{1,0:T(8,128)S(1)}, u32[]{:S(2)}, u32[]{:S(2)}) collective-permute-start(f32[80,768]{1,0:T(8,128)S(1)} %collective-permute-done.6.refs_2_.refs_7_), channel_id=1, source_target_pairs={{0,8},{8,0},{16,24},{24,16},{1,9},{9,1},{17,25},{25,17},{2,10},{10... | collective-permute-start | bytes 737288 | tf_op jit(solution)/shard_map/ppermute | solution.py:21
  21.4 8.3 %collective-permute-start.3 = (f32[32,768]{1,0:T(8,128)S(1)}, f32[32,768]{1,0:T(8,128)S(1)}, u32[]{:S(2)}, u32[]{:S(2)}) collective-permute-start(f32[32,768]{1,0:T(8,128)S(1)} %add_add_fusion), channel_id=1, source_target_pairs={{0,8},{8,0},{16,24},{24,16},{1,9},{9,1},{17,25},{25,17},{2,10},{10... | collective-permute-start | bytes 294920 | tf_op jit(solution)/shard_map/ppermute | solution.py:21
  29.8 6.4 %collective-permute-start.4 = (f32[32,768]{1,0:T(8,128)S(1)}, f32[32,768]{1,0:T(8,128)S(1)}, u32[]{:S(2)}, u32[]{:S(2)}) collective-permute-start(f32[32,768]{1,0:T(8,128)S(1)} %add.18.mine.refs_7_), channel_id=1, source_target_pairs={{0,16},{8,24},{16,0},{24,8},{1,17},{9,25},{17,1},{25,9},{2,18},{10... | collective-permute-start | bytes 294920 | tf_op jit(solution)/shard_map/ppermute | solution.py:21
  36.9 5.6 %collective-permute-start.10 = (f32[32,768]{1,0:T(8,128)S(1)}, f32[32,768]{1,0:T(8,128)S(1)}, u32[]{:S(2)}, u32[]{:S(2)}) collective-permute-start(f32[32,768]{1,0:T(8,128)S(1)} %shard_map.188.refs_0_), channel_id=1, source_target_pairs={{0,6},{2,4},{4,2},{6,0},{1,7},{3,5},{5,3},{7,1},{8,14},{10,12},{12... | collective-permute-start | bytes 294920 | tf_op jit(solution)/shard_map/ppermute | solution.py:21
  36.9 6.1 %collective-permute-start.8 = (f32[32,768]{1,0:T(8,128)S(1)}, f32[32,768]{1,0:T(8,128)S(1)}, u32[]{:S(2)}, u32[]{:S(2)}) collective-permute-start(f32[32,768]{1,0:T(8,128)S(1)} %shard_map.188.refs_0_), channel_id=1, source_target_pairs={{0,2},{2,0},{4,6},{6,4},{1,3},{3,1},{5,7},{7,5},{8,10},{10,8},{12,... | collective-permute-start | bytes 294920 | tf_op jit(solution)/shard_map/ppermute | solution.py:21
  38.1 5.4 %collective-permute-start.9 = (f32[32,768]{1,0:T(8,128)S(1)}, f32[32,768]{1,0:T(8,128)S(1)}, u32[]{:S(2)}, u32[]{:S(2)}) collective-permute-start(f32[32,768]{1,0:T(8,128)S(1)} %shard_map.188.refs_0_), channel_id=1, source_target_pairs={{0,4},{2,6},{4,0},{6,2},{1,5},{3,7},{5,1},{7,3},{8,12},{10,14},{12... | collective-permute-start | bytes 294920 | tf_op jit(solution)/shard_map/ppermute | solution.py:21
  40.4 5.7 %collective-permute-start.17 = (f32[64,768]{1,0:T(8,128)S(1)}, f32[64,768]{1,0:T(8,128)S(1)}, u32[]{:S(2)}, u32[]{:S(2)}) collective-permute-start(f32[64,768]{1,0:T(8,128)S(1)} %slice.33), channel_id=1, source_target_pairs={{0,2},{2,0},{4,6},{6,4},{1,3},{3,1},{5,7},{7,5},{8,10},{10,8},{12,... | collective-permute-start | bytes 589832 | tf_op jit(solution)/shard_map/ppermute | solution.py:21
  40.5 5.9 %collective-permute-start.18 = (f32[64,768]{1,0:T(8,128)S(1)}, f32[64,768]{1,0:T(8,128)S(1)}, u32[]{:S(2)}, u32[]{:S(2)}) collective-permute-start(f32[64,768]{1,0:T(8,128)S(1)} %slice.33), channel_id=1, source_target_pairs={{0,4},{2,6},{4,0},{6,2},{1,5},{3,7},{5,1},{7,3},{8,12},{10,14},{12... | collective-permute-start | bytes 589832 | tf_op jit(solution)/shard_map/ppermute | solution.py:21
  44.2 4.0 %collective-permute-start.11 = (f32[2,128]{1,0:T(2,128)S(1)}, f32[2,128]{1,0:T(2,128)S(1)}, u32[]{:S(2)}, u32[]{:S(2)}) collective-permute-start(f32[2,128]{1,0:T(2,128)S(1)} %get-tuple-element.37), channel_id=1, source_target_pairs={{0,1},{1,0},{2,3},{3,2},{4,5},{5,4},{6,7},{7,6},{8,9},{9,8},{10,11... | collective-permute-start | bytes 3080 | tf_op jit(solution)/shard_map/ppermute | solution.py:21
  44.3 8.5 %collective-permute-start.16 = (f32[64,768]{1,0:T(8,128)S(1)}, f32[64,768]{1,0:T(8,128)S(1)}, u32[]{:S(2)}, u32[]{:S(2)}) collective-permute-start(f32[64,768]{1,0:T(8,128)S(1)} %pad_maximum_fusion.2.refs_2_), channel_id=1, source_target_pairs={{0,8},{8,0},{16,24},{24,16},{1,9},{9,1},{17,25},{25,17},{2,10},{10... | collective-permute-start | bytes 589832 | tf_op jit(solution)/shard_map/ppermute | solution.py:21
  44.7 9.0 %collective-permute-start.20 = (f32[64,768]{1,0:T(8,128)S(1)}, f32[64,768]{1,0:T(8,128)S(1)}, u32[]{:S(2)}, u32[]{:S(2)}) collective-permute-start(f32[64,768]{1,0:T(8,128)S(1)} %slice.34), channel_id=1, source_target_pairs={{0,2},{2,0},{4,6},{6,4},{1,3},{3,1},{5,7},{7,5},{8,10},{10,8},{12,... | collective-permute-start | bytes 589832 | tf_op jit(solution)/shard_map/ppermute | solution.py:21
  46.2 11.0 %collective-permute-start.21 = (f32[64,768]{1,0:T(8,128)S(1)}, f32[64,768]{1,0:T(8,128)S(1)}, u32[]{:S(2)}, u32[]{:S(2)}) collective-permute-start(f32[64,768]{1,0:T(8,128)S(1)} %slice.34), channel_id=1, source_target_pairs={{0,4},{2,6},{4,0},{6,2},{1,5},{3,7},{5,1},{7,3},{8,12},{10,14},{12... | collective-permute-start | bytes 589832 | tf_op jit(solution)/shard_map/ppermute | solution.py:21
  46.5 10.7 %collective-permute-start.22 = (f32[64,768]{1,0:T(8,128)S(1)}, f32[64,768]{1,0:T(8,128)S(1)}, u32[]{:S(2)}, u32[]{:S(2)}) collective-permute-start(f32[64,768]{1,0:T(8,128)S(1)} %slice.34), channel_id=1, source_target_pairs={{0,6},{2,4},{4,2},{6,0},{1,7},{3,5},{5,3},{7,1},{8,14},{10,12},{12... | collective-permute-start | bytes 589832 | tf_op jit(solution)/shard_map/ppermute | solution.py:21
  48.2 11.8 %collective-permute-start.19 = (f32[64,768]{1,0:T(8,128)S(1)}, f32[64,768]{1,0:T(8,128)S(1)}, u32[]{:S(2)}, u32[]{:S(2)}) collective-permute-start(f32[64,768]{1,0:T(8,128)S(1)} %pad_maximum_fusion.2.refs_2_), channel_id=1, source_target_pairs={{0,16},{8,24},{16,0},{24,8},{1,17},{9,25},{17,1},{25,9},{2,18},{10... | collective-permute-start | bytes 589832 | tf_op jit(solution)/shard_map/ppermute | solution.py:21

commit v3 on v2

--- a/solution.py
+++ b/solution.py
@@ -84,11 +84,19 @@
     chunks, total = refs[:rep], refs[rep]
     r = place[1]
     query_width = query_cot.shape[1]
-    for basis, cot, lo in ((query_basis, query_cot, 0), (value_basis, value_cot, query_width)):
-        reduced = jnp.dot(tokens[...], basis[...], preferred_element_type=F32)
+    bases = jnp.concatenate([query_basis[...], value_basis[...]], axis=1)
+    both = jnp.dot(tokens[...], bases, preferred_element_type=F32)
+    rank = query_basis.shape[1]
+    for cot, lo, at in ((query_cot, 0, 0), (value_cot, query_width, rank)):
+        reduced = both[:, at : at + rank]
         high = reduced.astype(BF16)
         low = (reduced - high.astype(F32)).astype(BF16)
-        total[:, lo : lo + cot.shape[1]] = parts_product(high, low, cot[...])
+        total[:, lo : lo + cot.shape[1]] = lax.dot_general(
+            jnp.concatenate([high, low], axis=0),
+            jnp.concatenate([cot[...], cot[...]], axis=0),
+            (((0,), (0,)), ((), ())),
+            preferred_element_type=F32,
+        )
     for k in range(rep):
         for zz in range(fs):
             chunks[k][zz * ranks : (zz + 1) * ranks, :] = total[
@@ -137,8 +145,10 @@
         wide = whole[:, lo : lo + product.shape[1]]
         high = wide.astype(BF16)
         low = (wide - high.astype(F32)).astype(BF16)
-        product[...] = jnp.dot(basis[...], high, preferred_element_type=F32) + jnp.dot(
-            basis[...], low, preferred_element_type=F32
+        product[...] = jnp.dot(
+            jnp.concatenate([basis[...], basis[...]], axis=1),
+            jnp.concatenate([high, low], axis=0),
+            preferred_element_type=F32,
         )
 
 
@@ -147,73 +157,91 @@
 
 
 def early_kernel(counts, pieces, place, sums, query_product, value_product, *refs):
+    rep, rows, entries, blocks, ranks = counts
+    sources, (mine, other), refs = refs[:blocks], refs[blocks : blocks + 2], refs[blocks + 2 :]
+    outs, copy_outs, held, staged, sems = refs[:8], refs[8:10], refs[10:12], refs[12:20], refs[20]
+    z, r = place[0], place[1]
+    query_width = query_product.shape[1]
+    factors = scales(sums, entries)
+    copies = []
+
+    def send(source, target):
+        copies.append(pltpu.make_async_copy(source, target, sems.at[len(copies)]))
+        copies[-1].start()
+
+    def form(kz, kr, source, start, offset, size):
+        owner = (z ^ kz) * rep + (r ^ kr)
+        where = pl.ds(pl.multiple_of(owner * rows + offset, size), size)
+        lo = 0
+        for i, product in enumerate((query_product, value_product)):
+            step = product[where, :] * factors[i]
+            weight = sources[source][start : start + size, lo : lo + product.shape[1]] - 0.01 * step
+            held[i][where, :] = weight.astype(BF16)
+            lo += product.shape[1]
+            if kz == 0 and kr == 0:
+                staged[i][...] = step
+                staged[2 + i][...] = weight
+
+    for piece in pieces:
+        if piece[0] == 0:
+            form(*piece)
+        if piece[:2] == (0, 0):
+            base = sources[piece[2]]
+            where = aligned(z, ranks)
+            first, second, _ = moments(
+                mine[where, :] + other[where, :],
+                base[rows : rows + ranks, :],
+                base[rows + ranks : rows + 2 * ranks, :],
+            )
+            staged[4][...] = first[:, :query_width]
+            staged[5][...] = second[:, :query_width]
+            staged[6][...] = first[:, query_width:]
+            staged[7][...] = second[:, query_width:]
+            for source, target in zip(staged, outs):
+                send(source, target)
+    where = pl.ds(pl.multiple_of(z * rep * rows, rep * rows), rep * rows)
+    for source, target in zip(held, copy_outs):
+        send(source.at[where, :], target.at[where, :])
+    for piece in pieces:
+        if piece[0] != 0:
+            form(*piece)
+    for copy in copies:
+        copy.wait()
+
+
+def late_kernel(counts, ready, pieces, place, sums, query_product, value_product, *refs):
     rep, rows, entries, blocks = counts
-    sources, held = refs[:blocks], refs[blocks:]
+    early, sources, refs = refs[:2], refs[2 : 2 + blocks], refs[4 + blocks :]
+    copy_outs, held, sems = refs[:2], refs[2:4], refs[4]
     z, r = place[0], place[1]
+    copies = []
+
+    def send(source, target):
+        copies.append(pltpu.make_async_copy(source, target, sems.at[len(copies)]))
+        copies[-1].start()
+
+    for kz in sorted({kz for kz, _ in ready}):
+        if all((kz, kr) in ready for kr in range(rep)):
+            groups = [pl.ds(pl.multiple_of((z ^ kz) * rep * rows, rep * rows), rep * rows)]
+        else:
+            groups = [
+                aligned((z ^ kz) * rep + (r ^ kr), rows) for kr in range(rep) if (kz, kr) in ready
+            ]
+        for where in groups:
+            for source, target in zip(early, copy_outs):
+                send(source.at[where, :], target.at[where, :])
     factors = scales(sums, entries)
     filled = 0
     for kz, kr, source, start, offset, size in pieces:
         owner = (z ^ kz) * rep + (r ^ kr)
         where = pl.ds(pl.multiple_of(owner * rows + offset, size), size)
         lo = 0
-        for product, factor, out in zip((query_product, value_product), factors, held):
+        for i, product in enumerate((query_product, value_product)):
             old = sources[source][start : start + size, lo : lo + product.shape[1]]
-            weight = old - 0.01 * (product[where, :] * factor)
-            out[filled : filled + size, :] = weight.astype(BF16)
-            lo += product.shape[1]
-        filled += size
-
-
-def late_kernel(counts, ready, pieces, place, sums, query_product, value_product, *refs):
-    rep, rows, entries, blocks, ranks = counts
-    early, sources, (mine, other) = refs[:2], refs[2 : 2 + blocks], refs[2 + blocks : 4 + blocks]
-    outs, refs = refs[4 + blocks : 14 + blocks], refs[14 + blocks :]
-    copy_outs, (held, staged, sems) = outs[8:], (refs[:2], refs[2:10], refs[10])
-    z, r = place[0], place[1]
-    query_width = query_product.shape[1]
-    copies = []
-
-    def send(source, target):
-        copies.append(pltpu.make_async_copy(source, target, sems.at[len(copies)]))
-        copies[-1].start()
-
-    def target_rows(kz, kr, offset, size):
-        owner = (z ^ kz) * rep + (r ^ kr)
-        return pl.ds(pl.multiple_of(owner * rows + offset, size), size)
-
-    filled = 0
-    for kz, kr, _, _, offset, size in ready:
-        for source, out in zip(early, copy_outs):
-            send(source.at[pl.ds(filled, size), :], out.at[target_rows(kz, kr, offset, size), :])
-        filled += size
-    factors = scales(sums, entries)
-    filled = 0
-    for kz, kr, source, start, offset, size in pieces:
-        where = target_rows(kz, kr, offset, size)
-        lo = 0
-        for i, product in enumerate((query_product, value_product)):
-            step = product[where, :] * factors[i]
-            weight = sources[source][start : start + size, lo : lo + product.shape[1]] - 0.01 * step
+            weight = old - 0.01 * (product[where, :] * factors[i])
             held[i][filled : filled + size, :] = weight.astype(BF16)
             send(held[i].at[pl.ds(filled, size), :], copy_outs[i].at[where, :])
             lo += product.shape[1]
-            if kz == 0 and kr == 0:
-                staged[i][...] = step
-                staged[2 + i][...] = weight
-                send(staged[i], outs[i])
-                send(staged[2 + i], outs[2 + i])
-        if kz == 0 and kr == 0:
-            where = aligned(z, ranks)
-            first, second, _ = moments(
-                mine[where, :] + other[where, :],
-                sources[source][rows : rows + ranks, :],
-                sources[source][rows + ranks : rows + 2 * ranks, :],
-            )
-            parts = (first[:, :query_width], second[:, :query_width])
-            parts += (first[:, query_width:], second[:, query_width:])
-            for i, part in enumerate(parts):
-                staged[4 + i][...] = part
-                send(staged[4 + i], outs[4 + i])
         filled += size
     for copy in copies:
         copy.wait()
@@ -353,7 +381,7 @@
         found = [[i for i, s in enumerate(sources) if s is piece[2]][0] for piece in pieces]
         return sources, [(p[0], p[1], i, *p[3:]) for p, i in zip(pieces, found)]
 
-    early, late = [], [(0, 0, own, 0, 0, rows)]
+    early, late = [(0, 0, own, 0, 0, rows)], []
     for kz in range(fs):
         group = late if kz == fs - 1 else early
         if kz > 0:
@@ -363,39 +391,49 @@
         if kz == fs - 1:
             late.append((kz, 3, far[kz][2], 0, 0, rows))
         else:
-            (late if kz == fs - 2 else early).append((kz, 3, ([cross] + crosses)[kz], 0, 0, rows))
+            (late if 0 < kz else early).append((kz, 3, ([cross] + crosses)[kz], 0, 0, rows))
 
     def halves(count, dtype=F32):
         return (shape(count, query_width, dtype=dtype), shape(count, value_width, dtype=dtype))
 
     sources, early = indexed(early)
-    early_rows = sum(piece[-1] for piece in early)
-    ready = call(
-        functools.partial(early_kernel, (rep, rows, entries, len(sources)), early),
-        halves(early_rows, BF16),
+    moment_shapes = (shape(ranks, query_width),) * 2 + (shape(ranks, value_width),) * 2
+    shapes = halves(rows) * 2 + moment_shapes
+    *outs, query_copy, value_copy, query_ready, value_ready = call(
+        functools.partial(early_kernel, (rep, rows, entries, len(sources), ranks), early),
+        shapes + halves(total, BF16) * 2,
         place,
         sums,
         *products,
         *sources,
+        mine,
+        other,
+        scratch=[pltpu.VMEM(s.shape, s.dtype) for s in shapes]
+        + [pltpu.SemaphoreType.DMA((10,))],
+        outside_out=range(10),
     )
     sources, late = indexed(late)
-    moment_shapes = (shape(ranks, query_width),) * 2 + (shape(ranks, value_width),) * 2
-    shapes = halves(rows) * 2 + moment_shapes
     late_rows = sum(piece[-1] for piece in late)
-    return call(
-        functools.partial(late_kernel, (rep, rows, entries, len(sources), ranks), early, late),
-        shapes + halves(total, BF16),
+    ready = frozenset(piece[:2] for piece in early if piece[0] > 0)
+    last = 6 + len(sources)
+    copies = call(
+        functools.partial(late_kernel, (rep, rows, entries, len(sources)), ready, late),
+        halves(total, BF16),
         place,
         sums,
         *products,
-        *ready,
+        query_ready,
+        value_ready,
         *sources,
-        mine,
-        other,
-        scratch=[pltpu.VMEM(s.shape, s.dtype) for s in halves(late_rows, BF16) + shapes]
-        + [pltpu.SemaphoreType.DMA((2 * len(early) + 2 * len(late) + 8,))],
-        outside_out=range(10),
-    )
+        query_copy,
+        value_copy,
+        scratch=[pltpu.VMEM(s.shape, s.dtype) for s in halves(late_rows, BF16)]
+        + [pltpu.SemaphoreType.DMA((2 * fs * rep,))],
+        outside=(last, last + 1),
+        outside_out=(0, 1),
+        aliases={last: 0, last + 1: 1},
+    )
+    return (*outs, *copies)
 
 
 def plain_body(

time: 62.3 us -> 62.3 us (level)
  no operation moved by 1% of the time
where the time goes in v3:
time: 62.3 us; the launch traced here: 62.2 us
  starting transfers between devices  30.2 us (48%)
  waiting for transfers between devices  23 us (37%)
  Pallas kernels  7.97 us (13%)
  between operations  0.83 us (1%)
    ppermute x23, starting transfers between devices, swap(): return lax.ppermute(block, axis, pairs)  30.2 us
    ppermute x23, waiting for transfers between devices, swap(): return lax.ppermute(block, axis, pairs)  23 us
    pallas_call x7, Pallas kernels, call(): pl.pallas_call(kernel, out_shape=out_shape, in_specs=specs, out_specs=tup...  7.97 us
  transfers between devices with their start and end apart: 23, of which 10 were waited for; matrix products, arithmetic and copies ran while one was open for 0% of the time, Pallas kernels for 7%

profile of v3, /device:TPU:0, one launch (start us, length us, event | category | flops | bytes accessed | tf_op | source)
XLA Modules:
  0.0 62.2 jit_solution(13266344761898619878)
XLA Ops:
  0.6 1.5 %shard_map.186 = (f32[64,768]{1,0:T(8,128)S(1)}, f32[80,768]{1,0:T(8,128)S(1)}, bf16[128,1024]{1,0:T(8,128)(2,1)S(1)}, bf16[1024,128]{1,0:T(8,128)(2,1)S(1)}, bf...) custom-call(f32[64,256]{1,0:T(8,128)} %refs_0_.1, f32[64,512]{1,0:T(8,128)} %refs_1_.1, ...), custom_call_target="tpu_custom_call" | custom-call | tf_op jit(solution)/shard_map/pallas_call | solution.py:280
  2.2 3.1 %collective-permute-start.5 = (f32[80,768]{1,0:T(8,128)S(1)}, f32[80,768]{1,0:T(8,128)S(1)}, u32[]{:S(2)}, u32[]{:S(2)}) collective-permute-start(f32[80,768]{1,0:T(8,128)S(1)} %get-tuple-element.48.refs_0_), channel_id=1, source_target_pairs={{0,8},{8,0},{16,24},{24,16},{1,9},{9,1},{17,25},{25,17},{2,10},{10... | collective-permute-start | bytes 737288 | tf_op jit(solution)/shard_map/ppermute | solution.py:21
  5.3 1.5 %collective-permute-start.12 = (f32[64,768]{1,0:T(8,128)S(1)}, f32[64,768]{1,0:T(8,128)S(1)}, u32[]{:S(2)}, u32[]{:S(2)}) collective-permute-start(f32[64,768]{1,0:T(8,128)S(1)} %get-tuple-element.53), channel_id=1, source_target_pairs={{0,2},{2,0},{4,6},{6,4},{1,3},{3,1},{5,7},{7,5},{8,10},{10,8},{12,... | collective-permute-start | bytes 589832 | tf_op jit(solution)/shard_map/ppermute | solution.py:21
  6.8 1.5 %collective-permute-start.13 = (f32[64,768]{1,0:T(8,128)S(1)}, f32[64,768]{1,0:T(8,128)S(1)}, u32[]{:S(2)}, u32[]{:S(2)}) collective-permute-start(f32[64,768]{1,0:T(8,128)S(1)} %get-tuple-element.53), channel_id=1, source_target_pairs={{0,4},{2,6},{4,0},{6,2},{1,5},{3,7},{5,1},{7,3},{8,12},{10,14},{12... | collective-permute-start | bytes 589832 | tf_op jit(solution)/shard_map/ppermute | solution.py:21
  8.3 2.6 %collective-permute-start.6 = (f32[80,768]{1,0:T(8,128)S(1)}, f32[80,768]{1,0:T(8,128)S(1)}, u32[]{:S(2)}, u32[]{:S(2)}) collective-permute-start(f32[80,768]{1,0:T(8,128)S(1)} %get-tuple-element.48.refs_0_), channel_id=1, source_target_pairs={{0,16},{8,24},{16,0},{24,8},{1,17},{9,25},{17,1},{25,9},{2,18},{10... | collective-permute-start | bytes 737288 | tf_op jit(solution)/shard_map/ppermute | solution.py:21
  10.9 0.1 pad_add_fusion.place
  11.0 1.1 %shard_map.187 = (f32[32,768]{1,0:T(8,128)S(1)}, f32[32,768]{1,0:T(8,128)S(1)}, f32[32,768]{1,0:T(8,128)S(1)}, f32[32,768]{1,0:T(8,128)S(1)}) custom-call(s32[2]{0:T(128)S(1)} %pad_add_fusion.place, bf16[128,1024]{1,0:T(8,128)(2,1)S(1)} %get-tuple-element.39.tokens, bf16[1024,128]{1,0:T(8,128)(2,1)S(1)} %get-tuple-element.40.query_basis, ...), custom_call_target="tpu_custom_call" | custom-call | tf_op jit(solution)/shard_map/pallas_call | solution.py:280
  12.1 0.6 collective-permute-start
  12.7 0.0 collective-permute-done.12.refs_1_
  12.7 0.5 collective-permute-start.1
  13.2 0.0 collective-permute-done.13.refs_2_
  13.2 2.5 %collective-permute-start.2 = (f32[32,768]{1,0:T(8,128)S(1)}, f32[32,768]{1,0:T(8,128)S(1)}, u32[]{:S(2)}, u32[]{:S(2)}) collective-permute-start(f32[32,768]{1,0:T(8,128)S(1)} %get-tuple-element.47), channel_id=1, source_target_pairs={{0,6},{2,4},{4,2},{6,0},{1,7},{3,5},{5,3},{7,1},{8,14},{10,12},{12... | collective-permute-start | bytes 294920 | tf_op jit(solution)/shard_map/ppermute | solution.py:21
  15.7 0.0 collective-permute-done.5.refs_1_.refs_4_
  15.8 1.0 %collective-permute-start.14 = (f32[96,768]{1,0:T(8,128)S(1)}, f32[96,768]{1,0:T(8,128)S(1)}, u32[]{:S(2)}, u32[]{:S(2)}) collective-permute-start(f32[96,768]{1,0:T(8,128)S(1)} %get-tuple-element.68), channel_id=1, source_target_pairs={{0,4},{2,6},{4,0},{6,2},{1,5},{3,7},{5,1},{7,3},{8,12},{10,14},{12... | collective-permute-start | bytes 884744 | tf_op jit(solution)/shard_map/ppermute | solution.py:21
  16.8 0.3 collective-permute-done
  17.1 2.1 %collective-permute-start.15 = (f32[96,768]{1,0:T(8,128)S(1)}, f32[96,768]{1,0:T(8,128)S(1)}, u32[]{:S(2)}, u32[]{:S(2)}) collective-permute-start(f32[96,768]{1,0:T(8,128)S(1)} %get-tuple-element.69), channel_id=1, source_target_pairs={{0,2},{2,0},{4,6},{6,4},{1,3},{3,1},{5,7},{7,5},{8,10},{10,8},{12,... | collective-permute-start | bytes 884744 | tf_op jit(solution)/shard_map/ppermute | solution.py:21
  19.2 2.1 %collective-permute-done.6.refs_2_.refs_7_ = f32[80,768]{1,0:T(8,128)S(1)} collective-permute-done((f32[80,768]{1,0:T(8,128)S(1)}, f32[80,768]{1,0:T(8,128)S(1)}, u32[]{:S(2)}, u32[]{:S(2)}) %collective-permute-start.6) | collective-permute-done | bytes 245792 | tf_op jit(solution)/shard_map/ppermute | solution.py:21
  21.4 0.0 collective-permute-start.7
  21.4 0.0 collective-permute-done.1
  21.4 0.0 collective-permute-done.2
  21.4 2.1 %collective-permute-start.3 = (f32[32,768]{1,0:T(8,128)S(1)}, f32[32,768]{1,0:T(8,128)S(1)}, u32[]{:S(2)}, u32[]{:S(2)}) collective-permute-start(f32[32,768]{1,0:T(8,128)S(1)} %add_add_fusion), channel_id=1, source_target_pairs={{0,8},{8,0},{16,24},{24,16},{1,9},{9,1},{17,25},{25,17},{2,10},{10... | collective-permute-start | bytes 294920 | tf_op jit(solution)/shard_map/ppermute | solution.py:21
  23.5 6.2 %collective-permute-done.3 = f32[32,768]{1,0:T(8,128)S(1)} collective-permute-done((f32[32,768]{1,0:T(8,128)S(1)}, f32[32,768]{1,0:T(8,128)S(1)}, u32[]{:S(2)}, u32[]{:S(2)}) %collective-permute-start.3) | collective-permute-done | bytes 98336 | tf_op jit(solution)/shard_map/ppermute | solution.py:21
  29.8 1.6 %collective-permute-start.4 = (f32[32,768]{1,0:T(8,128)S(1)}, f32[32,768]{1,0:T(8,128)S(1)}, u32[]{:S(2)}, u32[]{:S(2)}) collective-permute-start(f32[32,768]{1,0:T(8,128)S(1)} %add.18.mine.refs_11_), channel_id=1, source_target_pairs={{0,16},{8,24},{16,0},{24,8},{1,17},{9,25},{17,1},{25,9},{2,18},{10... | collective-permute-start | bytes 294920 | tf_op jit(solution)/shard_map/ppermute | solution.py:21
  31.4 4.8 %collective-permute-done.4.other.refs_12_ = f32[32,768]{1,0:T(8,128)S(1)} collective-permute-done((f32[32,768]{1,0:T(8,128)S(1)}, f32[32,768]{1,0:T(8,128)S(1)}, u32[]{:S(2)}, u32[]{:S(2)}) %collective-permute-start.4) | collective-permute-done | bytes 98336 | tf_op jit(solution)/shard_map/ppermute | solution.py:21
  36.2 0.0 collective-permute-done.7.refs_3_.refs_10_
  36.2 0.6 shard_map.188.refs_0_
  36.9 0.1 collective-permute-start.10
  36.9 1.1 %collective-permute-start.8 = (f32[32,768]{1,0:T(8,128)S(1)}, f32[32,768]{1,0:T(8,128)S(1)}, u32[]{:S(2)}, u32[]{:S(2)}) collective-permute-start(f32[32,768]{1,0:T(8,128)S(1)} %shard_map.188.refs_0_), channel_id=1, source_target_pairs={{0,2},{2,0},{4,6},{6,4},{1,3},{3,1},{5,7},{7,5},{8,10},{10,8},{12,... | collective-permute-start | bytes 294920 | tf_op jit(solution)/shard_map/ppermute | solution.py:21
  38.1 2.3 %collective-permute-start.9 = (f32[32,768]{1,0:T(8,128)S(1)}, f32[32,768]{1,0:T(8,128)S(1)}, u32[]{:S(2)}, u32[]{:S(2)}) collective-permute-start(f32[32,768]{1,0:T(8,128)S(1)} %shard_map.188.refs_0_), channel_id=1, source_target_pairs={{0,4},{2,6},{4,0},{6,2},{1,5},{3,7},{5,1},{7,3},{8,12},{10,14},{12... | collective-permute-start | bytes 294920 | tf_op jit(solution)/shard_map/ppermute | solution.py:21
  40.4 0.0 collective-permute-done.14.refs_6_
  40.4 0.1 collective-permute-start.16
  40.5 0.0 collective-permute-done.15.refs_5_
  40.5 0.6 collective-permute-start.17
  41.2 2.3 %collective-permute-done.10.refs_3_ = f32[32,768]{1,0:T(8,128)S(1)} collective-permute-done((f32[32,768]{1,0:T(8,128)S(1)}, f32[32,768]{1,0:T(8,128)S(1)}, u32[]{:S(2)}, u32[]{:S(2)}) %collective-permute-start.10) | collective-permute-done | bytes 98336 | tf_op jit(solution)/shard_map/ppermute | solution.py:21
  43.5 0.0 collective-permute-start.20
  43.5 0.3 collective-permute-done.8.refs_1_
  43.8 2.2 %collective-permute-start.21 = (f32[64,768]{1,0:T(8,128)S(1)}, f32[64,768]{1,0:T(8,128)S(1)}, u32[]{:S(2)}, u32[]{:S(2)}) collective-permute-start(f32[64,768]{1,0:T(8,128)S(1)} %slice.34), channel_id=1, source_target_pairs={{0,4},{2,6},{4,0},{6,2},{1,5},{3,7},{5,1},{7,3},{8,12},{10,14},{12... | collective-permute-start | bytes 589832 | tf_op jit(solution)/shard_map/ppermute | solution.py:21
  46.0 0.0 collective-permute-done.9.refs_2_
  46.0 0.7 %shard_map.189 = (f32[128,768]{1,0:T(8,128)S(1)}, f32[2,128]{1,0:T(2,128)S(1)}) custom-call(s32[2]{0:T(128)S(1)} %pad_add_fusion.place, f32[32,768]{1,0:T(8,128)S(1)} %shard_map.188.refs_0_, f32[32,768]{1,0:T(8,128)S(1)} %collective-permute-done.8.refs_1_, f32[32,768]{1,0:T(8,128)S(1)} %collective-permute-done.9.refs_2_, ...), custom_call_target="tpu_custom_call" | custom-call | tf_op jit(solution)/shard_map/pallas_call | solution.py:280
  46.7 0.1 collective-permute-start.11
  46.8 0.4 collective-permute-done.16.refs_8_
  47.3 1.0 %collective-permute-start.22 = (f32[64,768]{1,0:T(8,128)S(1)}, f32[64,768]{1,0:T(8,128)S(1)}, u32[]{:S(2)}, u32[]{:S(2)}) collective-permute-start(f32[64,768]{1,0:T(8,128)S(1)} %slice.34), channel_id=1, source_target_pairs={{0,6},{2,4},{4,2},{6,0},{1,7},{3,5},{5,3},{7,1},{8,14},{10,12},{12... | collective-permute-start | bytes 589832 | tf_op jit(solution)/shard_map/ppermute | solution.py:21
  48.2 0.0 collective-permute-done.17.refs_9_
  48.2 0.5 collective-permute-start.18
  48.7 0.0 collective-permute-done.11
  48.7 3.1 %collective-permute-start.19 = (f32[64,768]{1,0:T(8,128)S(1)}, f32[64,768]{1,0:T(8,128)S(1)}, u32[]{:S(2)}, u32[]{:S(2)}) collective-permute-start(f32[64,768]{1,0:T(8,128)S(1)} %pad_maximum_fusion.2.refs_3_), channel_id=1, source_target_pairs={{0,16},{8,24},{16,0},{24,8},{1,17},{9,25},{17,1},{25,9},{2,18},{10... | collective-permute-start | bytes 589832 | tf_op jit(solution)/shard_map/ppermute | solution.py:21
  51.8 0.6 shard_map.190
  52.4 1.6 %shard_map.191 = (f32[64,256]{1,0:T(8,128)}, f32[64,512]{1,0:T(8,128)}, f32[64,256]{1,0:T(8,128)}, f32[64,512]{1,0:T(8,128)}, f32[8,256]{1,0:T(8,128)}, /*index=...) custom-call(s32[2]{0:T(128)S(1)} %pad_add_fusion.place, ...), custom_call_target="tpu_custom_call" | custom-call | tf_op jit(solution)/shard_map/pallas_call | solution.py:280
  54.0 0.0 collective-permute-done.20.refs_4_
  54.0 0.0 collective-permute-done.21.refs_5_
  54.0 1.1 %collective-permute-done.22.refs_6_ = f32[64,768]{1,0:T(8,128)S(1)} collective-permute-done((f32[64,768]{1,0:T(8,128)S(1)}, f32[64,768]{1,0:T(8,128)S(1)}, u32[]{:S(2)}, u32[]{:S(2)}) %collective-permute-start.22) | collective-permute-done | bytes 196640 | tf_op jit(solution)/shard_map/ppermute | solution.py:21
  55.1 3.8 %collective-permute-done.18.refs_2_ = f32[64,768]{1,0:T(8,128)S(1)} collective-permute-done((f32[64,768]{1,0:T(8,128)S(1)}, f32[64,768]{1,0:T(8,128)S(1)}, u32[]{:S(2)}, u32[]{:S(2)}) %collective-permute-start.18) | collective-permute-done | bytes 196640 | tf_op jit(solution)/shard_map/ppermute | solution.py:21
  58.9 1.5 %collective-permute-done.19.refs_3_ = f32[64,768]{1,0:T(8,128)S(1)} collective-permute-done((f32[64,768]{1,0:T(8,128)S(1)}, f32[64,768]{1,0:T(8,128)S(1)}, u32[]{:S(2)}, u32[]{:S(2)}) %collective-permute-start.19) | collective-permute-done | bytes 196640 | tf_op jit(solution)/shard_map/ppermute | solution.py:21
  60.4 1.8 %shard_map.192 = (bf16[1024,256]{1,0:T(8,128)(2,1)}, bf16[1024,512]{1,0:T(8,128)(2,1)}) custom-call(s32[2]{0:T(128)S(1)} %pad_add_fusion.place, f32[2,128]{1,0:T(2,128)S(1)} %add.19.sums, f32[1024,256]{1,0:T(8,128)S(1)} %get-tuple-element.51.query_product, ...), custom_call_target="tpu_custom_call", output_to_operand_aliasing={{0}: (11, {}), {1}: (12, {})} | custom-call | tf_op jit(solution)/shard_map/pallas_call | solution.py:280
  (12 shorter events, 0.2 us)
Async XLA Ops:
  2.2 13.6 %collective-permute-start.5 = (f32[80,768]{1,0:T(8,128)S(1)}, f32[80,768]{1,0:T(8,128)S(1)}, u32[]{:S(2)}, u32[]{:S(2)}) collective-permute-start(f32[80,768]{1,0:T(8,128)S(1)} %get-tuple-element.48.refs_0_), channel_id=1, source_target_pairs={{0,8},{8,0},{16,24},{24,16},{1,9},{9,1},{17,25},{25,17},{2,10},{10... | collective-permute-start | bytes 737288 | tf_op jit(solution)/shard_map/ppermute | solution.py:21
  5.3 7.4 %collective-permute-start.12 = (f32[64,768]{1,0:T(8,128)S(1)}, f32[64,768]{1,0:T(8,128)S(1)}, u32[]{:S(2)}, u32[]{:S(2)}) collective-permute-start(f32[64,768]{1,0:T(8,128)S(1)} %get-tuple-element.53), channel_id=1, source_target_pairs={{0,2},{2,0},{4,6},{6,4},{1,3},{3,1},{5,7},{7,5},{8,10},{10,8},{12,... | collective-permute-start | bytes 589832 | tf_op jit(solution)/shard_map/ppermute | solution.py:21
  6.8 6.4 %collective-permute-start.13 = (f32[64,768]{1,0:T(8,128)S(1)}, f32[64,768]{1,0:T(8,128)S(1)}, u32[]{:S(2)}, u32[]{:S(2)}) collective-permute-start(f32[64,768]{1,0:T(8,128)S(1)} %get-tuple-element.53), channel_id=1, source_target_pairs={{0,4},{2,6},{4,0},{6,2},{1,5},{3,7},{5,1},{7,3},{8,12},{10,14},{12... | collective-permute-start | bytes 589832 | tf_op jit(solution)/shard_map/ppermute | solution.py:21
  8.3 13.1 %collective-permute-start.6 = (f32[80,768]{1,0:T(8,128)S(1)}, f32[80,768]{1,0:T(8,128)S(1)}, u32[]{:S(2)}, u32[]{:S(2)}) collective-permute-start(f32[80,768]{1,0:T(8,128)S(1)} %get-tuple-element.48.refs_0_), channel_id=1, source_target_pairs={{0,16},{8,24},{16,0},{24,8},{1,17},{9,25},{17,1},{25,9},{2,18},{10... | collective-permute-start | bytes 737288 | tf_op jit(solution)/shard_map/ppermute | solution.py:21
  12.1 5.0 %collective-permute-start = (f32[32,768]{1,0:T(8,128)S(1)}, f32[32,768]{1,0:T(8,128)S(1)}, u32[]{:S(2)}, u32[]{:S(2)}) collective-permute-start(f32[32,768]{1,0:T(8,128)S(1)} %get-tuple-element.45), channel_id=1, source_target_pairs={{0,2},{2,0},{4,6},{6,4},{1,3},{3,1},{5,7},{7,5},{8,10},{10,8},{12,... | collective-permute-start | bytes 294920 | tf_op jit(solution)/shard_map/ppermute | solution.py:21
  12.7 8.7 %collective-permute-start.1 = (f32[32,768]{1,0:T(8,128)S(1)}, f32[32,768]{1,0:T(8,128)S(1)}, u32[]{:S(2)}, u32[]{:S(2)}) collective-permute-start(f32[32,768]{1,0:T(8,128)S(1)} %get-tuple-element.46), channel_id=1, source_target_pairs={{0,4},{2,6},{4,0},{6,2},{1,5},{3,7},{5,1},{7,3},{8,12},{10,14},{12... | collective-permute-start | bytes 294920 | tf_op jit(solution)/shard_map/ppermute | solution.py:21
  13.2 8.2 %collective-permute-start.2 = (f32[32,768]{1,0:T(8,128)S(1)}, f32[32,768]{1,0:T(8,128)S(1)}, u32[]{:S(2)}, u32[]{:S(2)}) collective-permute-start(f32[32,768]{1,0:T(8,128)S(1)} %get-tuple-element.47), channel_id=1, source_target_pairs={{0,6},{2,4},{4,2},{6,0},{1,7},{3,5},{5,3},{7,1},{8,14},{10,12},{12... | collective-permute-start | bytes 294920 | tf_op jit(solution)/shard_map/ppermute | solution.py:21
  15.8 24.6 %collective-permute-start.14 = (f32[96,768]{1,0:T(8,128)S(1)}, f32[96,768]{1,0:T(8,128)S(1)}, u32[]{:S(2)}, u32[]{:S(2)}) collective-permute-start(f32[96,768]{1,0:T(8,128)S(1)} %get-tuple-element.68), channel_id=1, source_target_pairs={{0,4},{2,6},{4,0},{6,2},{1,5},{3,7},{5,1},{7,3},{8,12},{10,14},{12... | collective-permute-start | bytes 884744 | tf_op jit(solution)/shard_map/ppermute | solution.py:21
  17.1 23.4 %collective-permute-start.15 = (f32[96,768]{1,0:T(8,128)S(1)}, f32[96,768]{1,0:T(8,128)S(1)}, u32[]{:S(2)}, u32[]{:S(2)}) collective-permute-start(f32[96,768]{1,0:T(8,128)S(1)} %get-tuple-element.69), channel_id=1, source_target_pairs={{0,2},{2,0},{4,6},{6,4},{1,3},{3,1},{5,7},{7,5},{8,10},{10,8},{12,... | collective-permute-start | bytes 884744 | tf_op jit(solution)/shard_map/ppermute | solution.py:21
  21.4 14.8 %collective-permute-start.7 = (f32[80,768]{1,0:T(8,128)S(1)}, f32[80,768]{1,0:T(8,128)S(1)}, u32[]{:S(2)}, u32[]{:S(2)}) collective-permute-start(f32[80,768]{1,0:T(8,128)S(1)} %collective-permute-done.6.refs_2_.refs_7_), channel_id=1, source_target_pairs={{0,8},{8,0},{16,24},{24,16},{1,9},{9,1},{17,25},{25,17},{2,10},{10... | collective-permute-start | bytes 737288 | tf_op jit(solution)/shard_map/ppermute | solution.py:21
  21.4 8.3 %collective-permute-start.3 = (f32[32,768]{1,0:T(8,128)S(1)}, f32[32,768]{1,0:T(8,128)S(1)}, u32[]{:S(2)}, u32[]{:S(2)}) collective-permute-start(f32[32,768]{1,0:T(8,128)S(1)} %add_add_fusion), channel_id=1, source_target_pairs={{0,8},{8,0},{16,24},{24,16},{1,9},{9,1},{17,25},{25,17},{2,10},{10... | collective-permute-start | bytes 294920 | tf_op jit(solution)/shard_map/ppermute | solution.py:21
  29.8 6.4 %collective-permute-start.4 = (f32[32,768]{1,0:T(8,128)S(1)}, f32[32,768]{1,0:T(8,128)S(1)}, u32[]{:S(2)}, u32[]{:S(2)}) collective-permute-start(f32[32,768]{1,0:T(8,128)S(1)} %add.18.mine.refs_11_), channel_id=1, source_target_pairs={{0,16},{8,24},{16,0},{24,8},{1,17},{9,25},{17,1},{25,9},{2,18},{10... | collective-permute-start | bytes 294920 | tf_op jit(solution)/shard_map/ppermute | solution.py:21
  36.9 6.6 %collective-permute-start.10 = (f32[32,768]{1,0:T(8,128)S(1)}, f32[32,768]{1,0:T(8,128)S(1)}, u32[]{:S(2)}, u32[]{:S(2)}) collective-permute-start(f32[32,768]{1,0:T(8,128)S(1)} %shard_map.188.refs_0_), channel_id=1, source_target_pairs={{0,6},{2,4},{4,2},{6,0},{1,7},{3,5},{5,3},{7,1},{8,14},{10,12},{12... | collective-permute-start | bytes 294920 | tf_op jit(solution)/shard_map/ppermute | solution.py:21
  36.9 6.9 %collective-permute-start.8 = (f32[32,768]{1,0:T(8,128)S(1)}, f32[32,768]{1,0:T(8,128)S(1)}, u32[]{:S(2)}, u32[]{:S(2)}) collective-permute-start(f32[32,768]{1,0:T(8,128)S(1)} %shard_map.188.refs_0_), channel_id=1, source_target_pairs={{0,2},{2,0},{4,6},{6,4},{1,3},{3,1},{5,7},{7,5},{8,10},{10,8},{12,... | collective-permute-start | bytes 294920 | tf_op jit(solution)/shard_map/ppermute | solution.py:21
  38.1 7.9 %collective-permute-start.9 = (f32[32,768]{1,0:T(8,128)S(1)}, f32[32,768]{1,0:T(8,128)S(1)}, u32[]{:S(2)}, u32[]{:S(2)}) collective-permute-start(f32[32,768]{1,0:T(8,128)S(1)} %shard_map.188.refs_0_), channel_id=1, source_target_pairs={{0,4},{2,6},{4,0},{6,2},{1,5},{3,7},{5,1},{7,3},{8,12},{10,14},{12... | collective-permute-start | bytes 294920 | tf_op jit(solution)/shard_map/ppermute | solution.py:21
  40.4 6.8 %collective-permute-start.16 = (f32[64,768]{1,0:T(8,128)S(1)}, f32[64,768]{1,0:T(8,128)S(1)}, u32[]{:S(2)}, u32[]{:S(2)}) collective-permute-start(f32[64,768]{1,0:T(8,128)S(1)} %slice.33), channel_id=1, source_target_pairs={{0,2},{2,0},{4,6},{6,4},{1,3},{3,1},{5,7},{7,5},{8,10},{10,8},{12,... | collective-permute-start | bytes 589832 | tf_op jit(solution)/shard_map/ppermute | solution.py:21
  40.5 7.7 %collective-permute-start.17 = (f32[64,768]{1,0:T(8,128)S(1)}, f32[64,768]{1,0:T(8,128)S(1)}, u32[]{:S(2)}, u32[]{:S(2)}) collective-permute-start(f32[64,768]{1,0:T(8,128)S(1)} %slice.33), channel_id=1, source_target_pairs={{0,4},{2,6},{4,0},{6,2},{1,5},{3,7},{5,1},{7,3},{8,12},{10,14},{12... | collective-permute-start | bytes 589832 | tf_op jit(solution)/shard_map/ppermute | solution.py:21
  43.5 10.5 %collective-permute-start.20 = (f32[64,768]{1,0:T(8,128)S(1)}, f32[64,768]{1,0:T(8,128)S(1)}, u32[]{:S(2)}, u32[]{:S(2)}) collective-permute-start(f32[64,768]{1,0:T(8,128)S(1)} %slice.34), channel_id=1, source_target_pairs={{0,2},{2,0},{4,6},{6,4},{1,3},{3,1},{5,7},{7,5},{8,10},{10,8},{12,... | collective-permute-start | bytes 589832 | tf_op jit(solution)/shard_map/ppermute | solution.py:21
  43.8 10.2 %collective-permute-start.21 = (f32[64,768]{1,0:T(8,128)S(1)}, f32[64,768]{1,0:T(8,128)S(1)}, u32[]{:S(2)}, u32[]{:S(2)}) collective-permute-start(f32[64,768]{1,0:T(8,128)S(1)} %slice.34), channel_id=1, source_target_pairs={{0,4},{2,6},{4,0},{6,2},{1,5},{3,7},{5,1},{7,3},{8,12},{10,14},{12... | collective-permute-start | bytes 589832 | tf_op jit(solution)/shard_map/ppermute | solution.py:21
  46.7 2.0 %collective-permute-start.11 = (f32[2,128]{1,0:T(2,128)S(1)}, f32[2,128]{1,0:T(2,128)S(1)}, u32[]{:S(2)}, u32[]{:S(2)}) collective-permute-start(f32[2,128]{1,0:T(2,128)S(1)} %get-tuple-element.49), channel_id=1, source_target_pairs={{0,1},{1,0},{2,3},{3,2},{4,5},{5,4},{6,7},{7,6},{8,9},{9,8},{10,11... | collective-permute-start | bytes 3080 | tf_op jit(solution)/shard_map/ppermute | solution.py:21
  47.3 7.8 %collective-permute-start.22 = (f32[64,768]{1,0:T(8,128)S(1)}, f32[64,768]{1,0:T(8,128)S(1)}, u32[]{:S(2)}, u32[]{:S(2)}) collective-permute-start(f32[64,768]{1,0:T(8,128)S(1)} %slice.34), channel_id=1, source_target_pairs={{0,6},{2,4},{4,2},{6,0},{1,7},{3,5},{5,3},{7,1},{8,14},{10,12},{12... | collective-permute-start | bytes 589832 | tf_op jit(solution)/shard_map/ppermute | solution.py:21
  48.2 10.7 %collective-permute-start.18 = (f32[64,768]{1,0:T(8,128)S(1)}, f32[64,768]{1,0:T(8,128)S(1)}, u32[]{:S(2)}, u32[]{:S(2)}) collective-permute-start(f32[64,768]{1,0:T(8,128)S(1)} %pad_maximum_fusion.2.refs_3_), channel_id=1, source_target_pairs={{0,8},{8,0},{16,24},{24,16},{1,9},{9,1},{17,25},{25,17},{2,10},{10... | collective-permute-start | bytes 589832 | tf_op jit(solution)/shard_map/ppermute | solution.py:21
  48.7 11.6 %collective-permute-start.19 = (f32[64,768]{1,0:T(8,128)S(1)}, f32[64,768]{1,0:T(8,128)S(1)}, u32[]{:S(2)}, u32[]{:S(2)}) collective-permute-start(f32[64,768]{1,0:T(8,128)S(1)} %pad_maximum_fusion.2.refs_3_), channel_id=1, source_target_pairs={{0,16},{8,24},{16,0},{24,8},{1,17},{9,25},{17,1},{25,9},{2,18},{10... | collective-permute-start | bytes 589832 | tf_op jit(solution)/shard_map/ppermute | solution.py:21
